TPU v7x, 256 devices: a whole 4x4x8 slice. The times are simulated.
256 devices in a mesh: sp: 32 (over z, x), tp: 8 (over y, core).
Axes of the slice: x: 4, y: 4, z: 8, core: 2. Of those that a mesh axis runs over, the one named last changes fastest.
Arguments:
- features: bfloat16 [12288, 2048], P('sp', 'tp'), may hold values from -6 to 6
- norm_gain: float32 [2048], replicated, may hold values from 0.28 to 10
- w_query: bfloat16 [2048, 1024], P(None, 'tp'), may hold values from -0.125 to 0.125
- w_key: bfloat16 [2048, 512], P(None, 'tp'), may hold values from -0.125 to 0.125
- w_value: bfloat16 [2048, 512], P(None, 'tp'), may hold values from -0.125 to 0.125
- head_sinks: float32 [16], P('tp'), may hold values from 1 to 5
- w_query_latent: bfloat16 [2048, 512], replicated, may hold values from -0.125 to 0.125
- w_kv_latent: bfloat16 [2048, 512], replicated, may hold values from -0.125 to 0.125
- w_rope_key: bfloat16 [2048, 64], replicated, may hold values from -0.125 to 0.125
- query_latent_gain: float32 [512], replicated, may hold values from 0.28 to 10
- kv_latent_gain: float32 [512], replicated, may hold values from 0.28 to 10
- w_query_content: bfloat16 [512, 1024], P(None, 'tp'), may hold values from -0.25 to 0.25
- w_query_rotary: bfloat16 [512, 512], P(None, 'tp'), may hold values from -0.25 to 0.25
- w_key_up: bfloat16 [512, 1024], P(None, 'tp'), may hold values from -0.25 to 0.25
- w_value_up: bfloat16 [512, 1024], P(None, 'tp'), may hold values from -0.25 to 0.25
- w_branch_window: bfloat16 [1024, 2048], P('tp'), may hold values from -0.1875 to 0.1875
- w_branch_latent: bfloat16 [1024, 2048], P('tp'), may hold values from -0.1875 to 0.1875
- w_gate_window: bfloat16 [2048, 2048], P(None, 'tp'), may hold values from -0.125 to 0.125
- w_gate_latent: bfloat16 [2048, 2048], P(None, 'tp'), may hold values from -0.125 to 0.125
Outputs:
- mixed: bfloat16 [12288, 2048], P('sp', 'tp')
All inputs are finite; a program needn't handle non-finite values.
Results may differ from a plain program's by a relative error of at most 0.018.
The roundings to bfloat16 on the way count: a program that leaves them out, or rounds other values in their place, can miss the bound.
Values may be sent and summed in bfloat16 or wider, within the bound.
A program may use at most 128 MiB of HBM per device.

v0:
```python
import jax
import jax.numpy as jnp
from jax import lax
from jax.sharding import PartitionSpec as P

HEAD = 64
WINDOW = 128
NOPE = 128
ROPE = 64
VDIM = 128


EPS = 1e-06
THETA = 10000.0
NEGATIVE = -1e30


def copy_for_each(shard, axis):
    count = lax.axis_size(axis)
    return lax.all_to_all(
        jnp.broadcast_to(shard[None], (count, *shard.shape)), axis, 0, 0, tiled=True
    )


def in_order(parts, dim):
    shape = list(parts.shape[1:])
    shape[dim] *= parts.shape[0]
    return jnp.moveaxis(parts, 0, dim).reshape(shape)


def gathered_copies(shard, axis, dim):
    parts = copy_for_each(shard, axis)
    return in_order(parts, dim)


def from_behind(shard, axis, by):
    count = lax.axis_size(axis)
    pairs = [(i, i + by) for i in range(count) if 0 <= i + by < count]
    return lax.ppermute(shard, axis, pairs)


def in_one_piece(arrays, axis, dim, along):
    widths = [a.shape[along] for a in arrays]
    both = jnp.concatenate(arrays, axis=along)
    result = lax.all_gather(both, axis, axis=dim, tiled=True)
    return tuple(jnp.split(result, [sum(widths[:k]) for k in range(1, len(widths))], axis=along))


def rms_rows(float_rows, gain_vec):
    return (
        float_rows
        * lax.rsqrt(jnp.mean(float_rows * float_rows, axis=-1, keepdims=True) + EPS)
        * gain_vec
    )


def rotate(float_rows, positions):
    half_width = float_rows.shape[-1] // 2
    frequencies = THETA ** (-jnp.arange(half_width, dtype=jnp.float32) / half_width)
    angles = positions.astype(jnp.float32)[:, None] * frequencies
    target = (float_rows.shape[0],) + (1,) * (float_rows.ndim - 2) + (half_width,)
    cosine = jnp.cos(angles).reshape(target)
    sine_part = jnp.sin(angles).reshape(target)
    first_half = float_rows[..., :half_width]
    second_half = float_rows[..., half_width:]
    return jnp.concatenate(
        [
            first_half * cosine - second_half * sine_part,
            second_half * cosine + first_half * sine_part,
        ],
        axis=-1,
    )


def project(left, right):
    return jnp.dot(left, right, preferred_element_type=jnp.float32)


def window_attention(queries, key_ext, value_ext, sink_table, row_start):
    row_count = queries.shape[0]
    kv_heads = key_ext.shape[1] // HEAD
    group_size = queries.shape[1] // HEAD // kv_heads
    blocks = row_count // WINDOW
    query_blocks = queries.reshape(blocks, WINDOW, kv_heads, group_size, HEAD)

    def banded(table):
        table = table.reshape(blocks + 1, WINDOW, kv_heads, HEAD)
        return jnp.concatenate([table[:-1], table[1:]], axis=1)

    key_band = banded(key_ext)
    value_band = banded(value_ext)
    scores = jnp.einsum(
        "nqhgd,nkhd->nhgqk", query_blocks, key_band, preferred_element_type=jnp.float32
    ) * HEAD ** (-0.5)
    query_index = jnp.arange(WINDOW, dtype=jnp.int32)[:, None]
    key_index = jnp.arange(2 * WINDOW, dtype=jnp.int32)[None, :]
    offset = query_index + WINDOW - key_index
    key_position = (
        row_start + jnp.arange(blocks, dtype=jnp.int32)[:, None, None] * WINDOW + key_index - WINDOW
    )
    valid_mask = ((offset >= 0) & (offset < WINDOW) & (key_position >= 0))[:, None, None]
    scores = jnp.where(valid_mask, scores, NEGATIVE)
    sink_logit = sink_table.reshape(1, kv_heads, group_size, 1, 1)
    row_top = jnp.maximum(jnp.max(scores, axis=-1, keepdims=True), sink_logit)
    weights = jnp.where(valid_mask, jnp.exp(scores - row_top), 0.0)
    denominator = jnp.sum(weights, axis=-1, keepdims=True) + jnp.exp(sink_logit - row_top)
    probabilities = (weights / denominator).astype(jnp.bfloat16)
    attended = jnp.einsum(
        "nhgqk,nkhd->nqhgd", probabilities, value_band, preferred_element_type=jnp.float32
    )
    return attended.astype(jnp.bfloat16).reshape(row_count, kv_heads * group_size * HEAD)


def on_device(
    features,
    norm_gain,
    w_query,
    w_key,
    w_value,
    head_sinks,
    w_query_latent,
    w_kv_latent,
    w_rope_key,
    query_latent_gain,
    kv_latent_gain,
    w_query_content,
    w_query_rotary,
    w_key_up,
    w_value_up,
    w_branch_window,
    w_branch_latent,
    w_gate_window,
    w_gate_latent,
):
    tok_rows = features.shape[0]
    row_start = lax.axis_index("sp") * tok_rows
    row_end = row_start + tok_rows
    positions = row_start + jnp.arange(tok_rows, dtype=jnp.int32)
    gathered = gathered_copies(features, "tp", 1)
    normed = rms_rows(gathered.astype(jnp.float32), norm_gain).astype(jnp.bfloat16)
    query_rows = project(normed, w_query).astype(jnp.bfloat16)
    key_rows = project(normed, w_key).astype(jnp.bfloat16)
    value_rows = project(normed, w_value).astype(jnp.bfloat16)
    key_width = key_rows.shape[1]
    packed = jnp.concatenate([key_rows, value_rows], axis=1)
    tail_rows = from_behind(packed[tok_rows - WINDOW :], "sp", 1)
    extended = jnp.concatenate([tail_rows, packed], axis=0)
    window_out = window_attention(
        query_rows, extended[:, :key_width], extended[:, key_width:], head_sinks, row_start
    )
    latent_query = rms_rows(project(normed, w_query_latent), query_latent_gain).astype(jnp.bfloat16)
    latent_kv = rms_rows(project(normed, w_kv_latent), kv_latent_gain).astype(jnp.bfloat16)
    rope_rows = rotate(project(normed, w_rope_key), positions).astype(jnp.bfloat16)
    lat_heads = w_key_up.shape[1] // NOPE
    query_content = (
        project(latent_query, w_query_content)
        .astype(jnp.bfloat16)
        .reshape(tok_rows, lat_heads, NOPE)
    )
    query_rotary = rotate(
        project(latent_query, w_query_rotary).reshape(tok_rows, lat_heads, ROPE), positions
    ).astype(jnp.bfloat16)
    scale_factor = (NOPE + ROPE) ** (-0.5)

    def attend(running, piece_keys, piece_values, rope_piece):
        running_max, denominator, accumulated = running
        piece_rows = piece_keys.shape[0]
        scores = (
            jnp.einsum(
                "qhd,khd->hqk",
                query_content,
                piece_keys.reshape(piece_rows, lat_heads, NOPE),
                preferred_element_type=jnp.float32,
            )
            + jnp.einsum(
                "qhr,kr->hqk", query_rotary, rope_piece, preferred_element_type=jnp.float32
            )
        ) * scale_factor
        key_position = jnp.arange(piece_rows, dtype=jnp.int32)
        live_mask = key_position[None, :] <= positions[:, None]
        scores = jnp.where(live_mask, scores, NEGATIVE)
        new_max = jnp.maximum(running_max, jnp.max(scores, axis=-1))
        weights = jnp.where(live_mask, jnp.exp(scores - new_max[..., None]), 0.0)
        denominator = jnp.sum(weights, axis=-1)
        accumulated = jnp.einsum(
            "hqk,khd->hqd",
            weights.astype(jnp.bfloat16),
            piece_values.reshape(piece_rows, lat_heads, VDIM),
            preferred_element_type=jnp.float32,
        )
        return (new_max, denominator, accumulated)

    initial = (
        jnp.full((lat_heads, tok_rows), NEGATIVE, jnp.float32),
        jnp.zeros((lat_heads, tok_rows), jnp.float32),
        jnp.zeros((lat_heads, tok_rows, VDIM), jnp.float32),
    )
    own_keys = project(latent_kv, w_key_up).astype(jnp.bfloat16)
    own_values = project(latent_kv, w_value_up).astype(jnp.bfloat16)
    pieces = in_one_piece((own_keys, own_values, rope_rows), "sp", 0, 1)
    running = lax.cond(
        jnp.int32(0) < row_end,
        lambda current: attend(current, pieces[0], pieces[1], pieces[2]),
        lambda current: current,
        initial,
    )
    latent_out = jnp.transpose(running[2] / running[1][..., None], (1, 0, 2))
    latent_out = latent_out.reshape(tok_rows, lat_heads * VDIM).astype(jnp.bfloat16)
    all_window, all_latent = in_one_piece((window_out, latent_out), "tp", 1, 0)
    column_window, column_latent = (
        lax.all_to_all(w_branch_window, "tp", split_axis=1, concat_axis=0, tiled=True),
        lax.all_to_all(w_branch_latent, "tp", split_axis=1, concat_axis=0, tiled=True),
    )
    window_branch = project(all_window, column_window)
    latent_branch = project(all_latent, column_latent)
    window_gate = jax.nn.sigmoid(project(normed, w_gate_window))
    latent_gate = jax.nn.sigmoid(project(normed, w_gate_latent))
    return (window_gate * window_branch + latent_gate * latent_branch).astype(jnp.bfloat16)


def solution(mesh):
    return jax.shard_map(
        on_device,
        mesh=mesh,
        in_specs=(
            P("sp", "tp"),
            P(),
            P(None, "tp"),
            P(None, "tp"),
            P(None, "tp"),
            P("tp"),
            P(),
            P(),
            P(),
            P(),
            P(),
            P(None, "tp"),
            P(None, "tp"),
            P(None, "tp"),
            P(None, "tp"),
            P("tp", None),
            P("tp", None),
            P(None, "tp"),
            P(None, "tp"),
        ),
        out_specs=P("sp", "tp"),
        check_vma=False,
    )
```

profile of v0, /device:TPU:3, one launch (start us, length us, event | category | flops | bytes accessed | tf_op | source)
XLA Modules:
  0.0 249.1 jit_solution(12856816892344930347)
XLA Ops:
  6.5 1.2 copy.42
  7.8 1.3 broadcast_in_dim.36
  9.1 5.1 %all-to-all-start = ((bf16[8,384,256]{1,2,0:T(8,128)(2,1)}), bf16[8,384,256]{1,2,0:T(8,128)(2,1)}, u32[]{:S(2)}, u32[]{:S(2)}) async-start(bf16[8,384,256]{1,2,0:T(8,128)(2,1)} %broadcast_in_dim.36), calls=%async_computation | async-start | bytes 3145728 | tf_op jit(solution)/shard_map/all_to_all | solution.py:20
  14.2 20.7 %all-to-all-done = bf16[8,384,256]{1,2,0:T(8,128)(2,1)} async-done(((bf16[8,384,256]{1,2,0:T(8,128)(2,1)}), bf16[8,384,256]{1,2,0:T(8,128)(2,1)}, u32[]{:S(2)}, u32[]{:S(2)}) %all-to-all-start) | async-done | bytes 1572896 | tf_op jit(solution)/shard_map/all_to_all | solution.py:20
  34.9 1.8 multiply_reduce_fusion
  36.7 1.8 fusion.19
  38.6 1.1 multiply_reduce_fusion.2
  41.2 0.7 pad_maximum_fusion
  42.3 1.9 convolution_convert_fusion.5
  44.3 1.8 convolution_convert_fusion.6
  46.1 3.3 %collective-permute-start = (bf16[128,128]{0,1:T(8,128)(2,1)S(1)}, bf16[128,128]{0,1:T(8,128)(2,1)S(1)}, u32[]{:S(2)}, u32[]{:S(2)}) collective-permute-start(bf16[128,128]{0,1:T(8,128)(2,1)S(1)} %pad_maximum_fusion.6), channel_id=1, source_target_pairs={{0,8},{8,16},{16,24},{24,32},{32,40},{40,48},{48,56},{56,64},{64,7... | collective-permute-start | bytes 98312 | tf_op jit(solution)/shard_map/ppermute | solution.py:39
  49.4 1.1 multiply_reduce_fusion.1
  51.5 0.6 convolution_convert_fusion.4
  53.6 85.6 %all-gather.3.cloned.1.call-done = bf16[12288,320]{0,1:T(8,128)(2,1)} async-done(((bf16[384,320]{0,1:T(8,128)(2,1)}), bf16[12288,320]{0,1:T(8,128)(2,1)}) %all-gather.3.cloned.1.call-update) | async-done | bytes 7864336 | tf_op jit(solution)/shard_map/all_gather | solution.py:45
  139.2 59.5 %conditional.1 = (f32[1,384]{1,0:T(1,128)S(1)}, f32[1,384,128]{1,2,0:T(8,128)S(1)}) conditional(s32[]{:T(128)} %convert_element_type.97, () %tuple.13, (s32[]{:T(128)}, s32[384]{0:T(512)S(1)}, bf16[12288,320]{0,1:T(8,128)(2,1)}, bf16[384,128]{1,0:T(8,128)(2,1)S(1)}, bf16[384,1,64]{0,2,1:T(8,128)(2,1)S(1)}) %tuple.14), branch_computations={%region_5.6_spmd, %region_6.9_spmd} | conditional | flops 3081240576 | bytes 119901712 | solution.py:201
  139.2 11.6 %copy.51 = bf16[12288,320]{1,0:T(8,128)(2,1)} copy(bf16[12288,320]{0,1:T(8,128)(2,1)} %get-tuple-element.44) | data formatting | bytes 15728640 | tf_op jit(solution)/shard_map
  150.8 9.8 %fusion.9 = f32[384,12288]{1,0:T(8,128)} fusion(bf16[384,128]{1,0:T(8,128)(2,1)S(1)} %get-tuple-element.25, bf16[12288,320]{1,0:T(8,128)(2,1)} %copy.51), kind=kOutput, calls=%fused_computation.11 | convolution fusion | flops 1207959552 | bytes 22118400 | tf_op jit(solution)/shard_map/cond/branch_1_fun/qhd,khd->hqk/dot_general | solution.py:169
  160.6 16.8 %fusion.63 = (f32[384]{0:T(512)S(1)}, f32[1,384,12288]{2,1,0:T(8,128)}) fusion(bf16[384,1,64]{0,2,1:T(8,128)(2,1)S(1)} %get-tuple-element.27, bf16[12288,320]{1,0:T(8,128)(2,1)} %copy.51, f32[384,12288]{1,0:T(8,128)} %fusion.9, s32[384]{0:T(512)S(1)} %broadcast_add_fusion), kind=kOutput, calls=%fused_computation.111 | convolution fusion | flops 627572352 | bytes 40946688 | tf_op jit(solution)/shard_map/cond/branch_1_fun/qhr,kr->hqk/dot_general | solution.py:175
  177.4 10.2 %fusion.11 = f32[1,384,128]{1,2,0:T(8,128)S(1)} fusion(bf16[12288,320]{1,0:T(8,128)(2,1)} %copy.51, f32[1,384,12288]{2,1,0:T(8,128)} %get-tuple-element.49, f32[384]{0:T(512)S(1)} %broadcast_maximum_fusion, s32[384]{0:T(512)S(1)} %broadcast_add_fusion), kind=kOutput, calls=%fused_computation.13 | convolution fusion | flops 1226833920 | bytes 22219776 | tf_op jit(solution)/shard_map/cond/branch_1_fun/hqk,khd->hqd/dot_general | solution.py:185
  187.6 11.1 %fusion.3 = f32[384]{0:T(512)S(1)} fusion(f32[1,384,12288]{2,1,0:T(8,128)} %get-tuple-element.49, f32[384]{0:T(512)S(1)} %broadcast_maximum_fusion, s32[384]{0:T(512)S(1)} %broadcast_add_fusion), kind=kLoop, calls=%fused_computation.6 | loop fusion | flops 18873984 | bytes 18878976 | tf_op jit(solution)/shard_map/cond/branch_1_fun/reduce_sum | solution.py:184
  198.8 0.7 pad_maximum_fusion.1
  199.5 1.0 copy.55
  200.5 8.0 %all-to-all-start.2 = ((bf16[128,8,256]{0,2,1:T(8,128)(2,1)}), bf16[128,8,256]{0,2,1:T(8,128)(2,1)S(1)}, u32[]{:S(2)}, u32[]{:S(2)}) async-start(bf16[128,8,256]{0,2,1:T(8,128)(2,1)} %bitcast.24), calls=%async_computation.2 | async-start | bytes 1048576 | tf_op jit(solution)/shard_map/all_to_all | solution.py:212
  208.5 1.0 copy.53
  209.5 8.3 %all-to-all-done.2 = bf16[128,8,256]{0,2,1:T(8,128)(2,1)S(1)} async-done(((bf16[128,8,256]{0,2,1:T(8,128)(2,1)}), bf16[128,8,256]{0,2,1:T(8,128)(2,1)S(1)}, u32[]{:S(2)}, u32[]{:S(2)}) %all-to-all-start.2) | async-done | bytes 524320 | tf_op jit(solution)/shard_map/all_to_all | solution.py:212
  217.9 4.4 %all-to-all-start.1 = ((bf16[128,8,256]{0,2,1:T(8,128)(2,1)}), bf16[128,8,256]{0,2,1:T(8,128)(2,1)S(1)}, u32[]{:S(2)}, u32[]{:S(2)}) async-start(bf16[128,8,256]{0,2,1:T(8,128)(2,1)} %bitcast.21), calls=%async_computation.1 | async-start | bytes 1048576 | tf_op jit(solution)/shard_map/all_to_all | solution.py:211
  222.5 10.0 %all-to-all-done.1 = bf16[128,8,256]{0,2,1:T(8,128)(2,1)S(1)} async-done(((bf16[128,8,256]{0,2,1:T(8,128)(2,1)}), bf16[128,8,256]{0,2,1:T(8,128)(2,1)S(1)}, u32[]{:S(2)}, u32[]{:S(2)}) %all-to-all-start.1) | async-done | bytes 524320 | tf_op jit(solution)/shard_map/all_to_all | solution.py:211
  232.5 1.0 copy.54
  233.5 2.7 %fusion.28 = f32[384,256]{1,0:T(8,128)} fusion(bf16[384,2048]{0,1:T(8,128)(2,1)S(1)} %copy-done.3, bf16[2048,256]{1,0:T(8,128)(2,1)} %param.39), kind=kOutput, calls=%fused_computation.35 | convolution fusion | flops 402948096 | bytes 3014656 | tf_op jit(solution)/shard_map/dot_general | solution.py:76
  236.2 2.2 fusion.25
  238.4 1.6 convolution_multiply_fusion.1
  240.1 2.2 fusion.29
  (91 shorter events, 4.4 us)
Async XLA Ops:
  6.5 32.0 %copy-start = (bf16[2048,512]{1,0:T(8,128)(2,1)S(1)}, bf16[2048,512]{1,0:T(8,128)(2,1)}, u32[]{:S(2)}) copy-start(bf16[2048,512]{1,0:T(8,128)(2,1)} %param.28) | copy-start | bytes 6291460
  7.8 28.9 %copy-start.15 = (f32[2048]{0:T(1024)S(1)}, f32[2048]{0:T(1024)}, u32[]{:S(2)}) copy-start(f32[2048]{0:T(1024)} %param.22) | copy-start | bytes 24580
  9.1 25.8 %all-to-all-start = ((bf16[8,384,256]{1,2,0:T(8,128)(2,1)}), bf16[8,384,256]{1,2,0:T(8,128)(2,1)}, u32[]{:S(2)}, u32[]{:S(2)}) async-start(bf16[8,384,256]{1,2,0:T(8,128)(2,1)} %broadcast_in_dim.36), calls=%async_computation | async-start | bytes 3145728 | tf_op jit(solution)/shard_map/all_to_all | solution.py:20
  14.2 125.0 %all-gather.3.cloned.1.call-start = ((), (), s32[]{:S(2)}) async-start(), calls=%async_computation.3 | async-start | bytes 8110080 | tf_op jit(solution)/shard_map/all_gather | solution.py:45
  38.6 2.0 copy-start.2
  38.6 1.2 copy-start.11
  38.6 1.2 copy-start.16
  38.6 1.5 copy-start.12
  38.6 1.9 copy-start.10
  39.7 2.6 %copy-start.8 = (bf16[2048,64]{0,1:T(8,128)(2,1)S(1)}, bf16[2048,64]{0,1:T(8,128)(2,1)}, u32[]{:S(2)}) copy-start(bf16[2048,64]{0,1:T(8,128)(2,1)} %param.25) | copy-start | bytes 786436
  40.2 4.1 %copy-start.9 = (bf16[2048,64]{0,1:T(8,128)(2,1)S(1)}, bf16[2048,64]{0,1:T(8,128)(2,1)}, u32[]{:S(2)}) copy-start(bf16[2048,64]{0,1:T(8,128)(2,1)} %param.24) | copy-start | bytes 786436
  40.9 8.4 %copy-start.3 = (bf16[384,2048]{0,1:T(8,128)(2,1)S(1)}, bf16[384,2048]{0,1:T(8,128)(2,1)}, u32[]{:S(2)}) copy-start(bf16[384,2048]{0,1:T(8,128)(2,1)} %copy-done.2) | copy-start | bytes 4718596
  42.0 196.5 %all-gather.5.cloned.1.call-start = ((), (), s32[]{:S(2)}) async-start(), calls=%async_computation.4 | async-start | bytes 1769472 | tf_op jit(solution)/shard_map/all_gather | solution.py:45
  42.0 7.4 %copy-start.19 = (bf16[2048,512]{1,0:T(8,128)(2,1)S(1)}, bf16[2048,512]{1,0:T(8,128)(2,1)}, u32[]{:S(2)}) copy-start(bf16[2048,512]{1,0:T(8,128)(2,1)} %param.27) | copy-start | bytes 6291460
  46.1 4.4 %copy-start.14 = (bf16[512,64]{0,1:T(8,128)(2,1)S(1)}, bf16[512,64]{0,1:T(8,128)(2,1)}, u32[]{:S(2)}) copy-start(bf16[512,64]{0,1:T(8,128)(2,1)} %param.33) | copy-start | bytes 196612
  46.1 4.4 %copy-start.17 = (f32[512]{0:T(512)S(1)}, f32[512]{0:T(512)}, u32[]{:S(2)}) copy-start(f32[512]{0:T(512)} %param.30) | copy-start | bytes 6148
  46.1 5.0 %copy-start.13 = (bf16[512,128]{1,0:T(8,128)(2,1)S(1)}, bf16[512,128]{1,0:T(8,128)(2,1)}, u32[]{:S(2)}) copy-start(bf16[512,128]{1,0:T(8,128)(2,1)} %param.32) | copy-start | bytes 393220
  46.1 5.4 %copy-start.7 = (bf16[2048,128]{1,0:T(8,128)(2,1)S(1)}, bf16[2048,128]{1,0:T(8,128)(2,1)}, u32[]{:S(2)}) copy-start(bf16[2048,128]{1,0:T(8,128)(2,1)} %param.23) | copy-start | bytes 1572868
  46.1 6.2 %collective-permute-start = (bf16[128,128]{0,1:T(8,128)(2,1)S(1)}, bf16[128,128]{0,1:T(8,128)(2,1)S(1)}, u32[]{:S(2)}, u32[]{:S(2)}) collective-permute-start(bf16[128,128]{0,1:T(8,128)(2,1)S(1)} %pad_maximum_fusion.6), channel_id=1, source_target_pairs={{0,8},{8,16},{16,24},{24,32},{32,40},{40,48},{48,56},{56,64},{64,7... | collective-permute-start | bytes 98312 | tf_op jit(solution)/shard_map/ppermute | solution.py:39
  51.2 1.6 copy-start.18
  139.2 60.3 %copy-start.4 = (bf16[128,2048]{1,0:T(8,128)(2,1)S(1)}, bf16[128,2048]{1,0:T(8,128)(2,1)}, u32[]{:S(2)}) copy-start(bf16[128,2048]{1,0:T(8,128)(2,1)} %param.37) | copy-start | bytes 1572868
  198.7 9.8 %copy-start.5 = (bf16[128,2048]{1,0:T(8,128)(2,1)S(1)}, bf16[128,2048]{1,0:T(8,128)(2,1)}, u32[]{:S(2)}) copy-start(bf16[128,2048]{1,0:T(8,128)(2,1)} %param.36) | copy-start | bytes 1572868
  200.5 17.3 %all-to-all-start.2 = ((bf16[128,8,256]{0,2,1:T(8,128)(2,1)}), bf16[128,8,256]{0,2,1:T(8,128)(2,1)S(1)}, u32[]{:S(2)}, u32[]{:S(2)}) async-start(bf16[128,8,256]{0,2,1:T(8,128)(2,1)} %bitcast.24), calls=%async_computation.2 | async-start | bytes 1048576 | tf_op jit(solution)/shard_map/all_to_all | solution.py:212
  217.9 14.6 %all-to-all-start.1 = ((bf16[128,8,256]{0,2,1:T(8,128)(2,1)}), bf16[128,8,256]{0,2,1:T(8,128)(2,1)S(1)}, u32[]{:S(2)}, u32[]{:S(2)}) async-start(bf16[128,8,256]{0,2,1:T(8,128)(2,1)} %bitcast.21), calls=%async_computation.1 | async-start | bytes 1048576 | tf_op jit(solution)/shard_map/all_to_all | solution.py:211
  233.5 2.7 %copy-start.20 = (bf16[2048,256]{1,0:T(8,128)(2,1)S(1)}, bf16[2048,256]{1,0:T(8,128)(2,1)}, u32[]{:S(2)}) copy-start(bf16[2048,256]{1,0:T(8,128)(2,1)} %param.38) | copy-start | bytes 3145732
  236.2 3.9 %copy-start.6 = (bf16[8,128,256]{2,1,0:T(8,128)(2,1)S(1)}, bf16[8,128,256]{2,1,0:T(8,128)(2,1)}, u32[]{:S(2)}) copy-start(bf16[8,128,256]{2,1,0:T(8,128)(2,1)} %copy.54) | copy-start | bytes 1572868
  236.2 6.1 %copy-start.1 = (bf16[2048,512]{1,0:T(8,128)(2,1)S(1)}, bf16[2048,512]{1,0:T(8,128)(2,1)}, u32[]{:S(2)}) copy-start(bf16[2048,512]{1,0:T(8,128)(2,1)} %param.28) | copy-start | bytes 6291460
Sparse Core Ops, SparseCore 0:
  42.1 97.0 all-gather.2
  199.6 31.8 all-gather.4
where the time goes:
time: 252 us; the launch traced here: 249 us
  waiting for transfers between devices  125 us (50%)
  matrix products  54.4 us (22%)
  starting transfers between devices  20.8 us (8%)
  local copies, waits for them, and re-layouts  17.9 us (7%)
  other arithmetic  17.4 us (7%)
  between operations  13.9 us (6%)
    all_gather x2, waiting for transfers between devices, in_one_piece(): result = lax.all_gather(both, axis, axis=dim, tiled=True)  85.7 us
    all_to_all x1, waiting for transfers between devices, copy_for_each(): lax.all_to_all(jnp.broadcast_to(shard[None], (count, *shard.shape)), axis...  20.7 us
    dot_general x14, matrix products, project(): return jnp.dot(left, right, preferred_element_type=jnp.float32)  17 us
    dot_general x1, matrix products, attend(): jnp.einsum('qhr,kr->hqk', query_rotary, rope_piece, preferred_element_typ...  16.8 us
    another operation x2, local copies, waits for them, and re-layouts  11.7 us
    reduce_sum x1, other arithmetic, attend(): denominator = jnp.sum(weights, axis=-1)  11.1 us
    dot_general x1, matrix products, attend(): jnp.einsum('hqk,khd->hqd', weights.astype(jnp.bfloat16), piece_values.res...  10.2 us
    all_to_all x1, waiting for transfers between devices, on_device(): lax.all_to_all(w_branch_window, 'tp', split_axis=1, concat_axis=0, tiled=...  10 us
  transfers between devices with their start and end apart: 6, of which 4 were waited for; matrix products, arithmetic and copies ran while one was open for 6% of the time, Pallas kernels for 0%

commit v1 on v0

v1 whole, which is shorter than its diff:
```python
import functools
import math

import jax
import jax.numpy as jnp
from jax import lax
from jax.experimental import pallas as pl
from jax.experimental.pallas import tpu as pltpu
from jax.sharding import PartitionSpec as P

D = 2048
HEAD = 64
WINDOW = 128
NOPE = 128
ROPE = 64
VDIM = 128
LATENT = 512
ROWS = 384
COLS = 256
NX = 4
NY = 4
NZ = 8
NTP = 8
NSP = 32
EPS = 1e-06
THETA = 10000.0
NEGATIVE = -1e30
SOFT = (NOPE + ROPE) ** (-0.5) * math.log2(math.e)
MESH = pl.DeviceIdType.MESH
F32 = jnp.float32
BF16 = jnp.bfloat16


def dot(a, b):
    return jnp.dot(a, b, preferred_element_type=F32)


def contract(a, b, da, db):
    return lax.dot_general(a, b, (((da,), (db,)), ((), ())), preferred_element_type=F32)


def layer(
    x_ref, gain_ref, table_ref, qgain_ref, kvgain_ref, sink_ref,
    wq_h, wk_h, wv_h, wql_h, wkvl_h, wr_h, wqc_h, wqr_h, wku_h, wvu_h, wbw_h, wbl_h, wgw_h, wgl_h,
    out_ref,
    feats, normed,
    wq, wk, wv, wql, wkvl, wr, wqc, wqr, wku, wvu, wgw, wgl,
    colw, coll, kbuf, rvbuf, qbuf, ext, qwin, gatew, gatel,
    m_s, l_s, acc, o_send, st_send, o_recv, st_recv, wout, lat,
    w_sem, fs_sem, fr_sem, ks_sem, kr_sem, vs_sem, vr_sem, qs_sem, qr_sem, ts_sem, tr_sem,
    bs_sem, br_sem, os_sem, or_sem, ss_sem, sr_sem, ws_sem, wr_sem, ls_sem, lr_sem,
):
    sp = lax.axis_index("sp")
    tp = lax.axis_index("tp")
    z = sp // NX
    x = sp % NX
    y = tp // 2
    c = tp % 2

    def z_peer(by):
        return (((z + by + NZ) % NZ) * NX + x, tp)

    def x_peer(by):
        return (z * NX + (x + by + NX) % NX, tp)

    def y_peer(by):
        return (sp, ((y + by + NY) % NY) * 2 + c)

    def tp_peer(by):
        return (sp, (tp + by + NTP) % NTP)

    def sp_peer(by):
        return ((sp + by + NSP) % NSP, tp)

    sibling = (sp, tp + 1 - 2 * c)

    def remote(src, dst, ssem, rsem, dev):
        return pltpu.make_async_remote_copy(
            src_ref=src, dst_ref=dst, send_sem=ssem, recv_sem=rsem, device_id=dev, device_id_type=MESH
        )

    own_cols = pl.ds(pl.multiple_of(tp * COLS, COLS), COLS)
    pairs = [
        (wkvl_h, wkvl), (wr_h, wr), (wku_h, wku), (wvu_h, wvu), (wql_h, wql), (wqc_h, wqc), (wqr_h, wqr),
        (wq_h, wq), (wk_h, wk), (wv_h, wv), (wgw_h, wgw), (wgl_h, wgl),
        (wbw_h.at[:, own_cols], colw.at[0]), (wbl_h.at[:, own_cols], coll.at[0]),
        (x_ref, feats.at[0]),
    ]
    loads = [pltpu.make_async_copy(a, b, w_sem.at[i]) for i, (a, b) in enumerate(pairs)]
    (L_KVL, L_R, L_KU, L_VU, L_QL, L_QC, L_QR, L_Q, L_K, L_V, L_GW, L_GL, L_BW, L_BL, L_X) = range(15)
    loads[L_X].start()
    for i in range(14):
        loads[i].start()

    barrier = pltpu.get_barrier_semaphore()
    partners = [z_peer(1), z_peer(-1), sp_peer(1), sp_peer(-1)]
    partners += [x_peer(d) for d in range(1, NX)]
    partners += [tp_peer(d) for d in range(1, NTP)]
    for dev in partners:
        pl.semaphore_signal(barrier, inc=1, device_id=dev, device_id_type=MESH)
    pl.semaphore_wait(barrier, len(partners))
    loads[L_X].wait()

    half = ROWS // 2
    top, bot = pl.ds(0, half), pl.ds(half, half)

    def feat(i, src, dst, dev):
        return remote(src, dst, fs_sem.at[i], fr_sem.at[i], dev)

    f_sib = feat(0, feats.at[0], feats.at[1], sibling)
    f_rt = feat(1, feats.at[0, top], feats.at[2, top], y_peer(1))
    f_rb = feat(2, feats.at[0, bot], feats.at[2, bot], y_peer(1))
    f_lb = feat(3, feats.at[0, bot], feats.at[6, bot], y_peer(-1))
    f_lt = feat(4, feats.at[0, top], feats.at[6, top], y_peer(-1))
    f_ft = feat(5, feats.at[2, top], feats.at[4, top], y_peer(1))
    f_fb = feat(6, feats.at[6, bot], feats.at[4, bot], y_peer(-1))
    h_lt = feat(7, feats.at[2, top], feats.at[3, top], sibling)
    h_lb = feat(8, feats.at[2, bot], feats.at[3, bot], sibling)
    h_rb = feat(9, feats.at[6, bot], feats.at[7, bot], sibling)
    h_rt = feat(10, feats.at[6, top], feats.at[7, top], sibling)
    h_ft = feat(11, feats.at[4, top], feats.at[5, top], sibling)
    h_fb = feat(12, feats.at[4, bot], feats.at[5, bot], sibling)
    for cp in (f_rt, f_lb, f_rb, f_lt, f_sib):
        cp.start()
    f_rt.wait_recv()
    f_ft.start()
    h_lt.start()
    f_lb.wait_recv()
    f_fb.start()
    h_rb.start()
    f_rb.wait_recv()
    h_lb.start()
    f_lt.wait_recv()
    h_rt.start()

    def squares(i):
        v = feats[i].astype(F32)
        v = v * v
        return v[:, :128] + v[:, 128:]

    f_sib.wait_recv()
    total = squares(0) + squares(1) + squares(2) + squares(6)
    h_lt.wait_recv()
    h_lb.wait_recv()
    h_rb.wait_recv()
    h_rt.wait_recv()
    total = total + squares(3) + squares(7)
    f_ft.wait_recv()
    h_ft.start()
    f_fb.wait_recv()
    h_fb.start()
    total = total + squares(4)
    h_ft.wait_recv()
    h_fb.wait_recv()
    total = total + squares(5)
    inv = lax.rsqrt(jnp.sum(total, axis=-1, keepdims=True) * (1.0 / D) + EPS)

    branch = []
    for d in range(1, NTP):
        peer = (tp + d) % NTP
        cols = pl.ds(pl.multiple_of(peer * COLS, COLS), COLS)
        branch.append(remote(wbw_h.at[:, cols], colw.at[d], bs_sem.at[d - 1], br_sem.at[d - 1], (sp, peer)))
        branch.append(remote(wbl_h.at[:, cols], coll.at[d], bs_sem.at[d + 6], br_sem.at[d + 6], (sp, peer)))
    for cp in branch:
        cp.start()

    for i in range(8):
        dy, dc = i // 2, i % 2
        src = ((y - dy + NY) % NY) * 2 + (c if dc == 0 else 1 - c)
        cols = pl.ds(pl.multiple_of(src * COLS, COLS), COLS)
        normed[:, cols] = (feats[i].astype(F32) * inv * gain_ref[:, cols]).astype(BF16)

    def rms(v, g):
        return (v * lax.rsqrt(jnp.mean(v * v, axis=-1, keepdims=True) + EPS) * g[...]).astype(BF16)

    cos_t = table_ref[0:32, :]
    sin_t = table_ref[32:64, :]

    def rotate_t(v):
        a, b = v[:32], v[32:]
        return jnp.concatenate([a * cos_t - b * sin_t, b * cos_t + a * sin_t], axis=0)

    loads[L_KVL].wait()
    loads[L_R].wait()
    loads[L_KU].wait()
    loads[L_VU].wait()
    lkv = rms(dot(normed[...], wkvl[...]), kvgain_ref)
    kbuf[0] = dot(lkv, wku[...]).astype(BF16)
    rvbuf[0, 64:192] = jnp.transpose(dot(lkv, wvu[...])).astype(BF16)
    rvbuf[0, 0:64] = rotate_t(jnp.transpose(dot(normed[...], wr[...]))).astype(BF16)

    def k_copy(i, src, dst, dev):
        return remote(kbuf.at[src], kbuf.at[dst], ks_sem.at[i], kr_sem.at[i], dev)

    def v_copy(i, src, dst, dev):
        return remote(rvbuf.at[src], rvbuf.at[dst], vs_sem.at[i], vr_sem.at[i], dev)

    up, down = z_peer(1), z_peer(-1)
    ups = [(0, 0, 1), (1, 1, 2), (2, 2, 3)]
    downs = [(3, 0, 4), (4, 4, 5), (5, 5, 6)]
    k_up = [k_copy(*t, up) for t in ups]
    v_up = [v_copy(*t, up) for t in ups]
    k_dn = [k_copy(*t, down) for t in downs]
    v_dn = [v_copy(*t, down) for t in downs]
    k_far = k_copy(6, 6, 7, down)
    v_far = v_copy(6, 3, 7, up)
    k_up[0].start()
    k_dn[0].start()
    v_up[0].start()
    v_dn[0].start()

    loads[L_QL].wait()
    loads[L_QC].wait()
    loads[L_QR].wait()
    lq = rms(dot(normed[...], wql[...]), qgain_ref)
    qbuf[0, 0:128] = jnp.transpose(dot(lq, wqc[...])).astype(BF16)
    qbuf[0, 128:192] = rotate_t(jnp.transpose(dot(lq, wqr[...]))).astype(BF16)
    q_cp = [
        remote(qbuf.at[0], qbuf.at[d], qs_sem.at[d - 1], qr_sem.at[d - 1], x_peer(d)) for d in range(1, NX)
    ]
    for cp in q_cp:
        cp.start()

    loads[L_Q].wait()
    loads[L_K].wait()
    loads[L_V].wait()
    w3 = jnp.concatenate([wq[...], wk[...], wv[...]], axis=1)
    rows3 = dot(normed[...], w3).astype(BF16)
    qwin[...] = rows3[:, :128]
    ext[WINDOW:, :] = rows3[:, 128:]
    tail = remote(ext.at[pl.ds(ROWS, WINDOW)], ext.at[pl.ds(0, WINDOW)], ts_sem, tr_sem, sp_peer(1))
    tail.start()

    loads[L_GW].wait()
    loads[L_GL].wait()
    gatew[...] = jax.nn.sigmoid(dot(normed[...], wgw[...]))
    gatel[...] = jax.nn.sigmoid(dot(normed[...], wgl[...]))

    tail.wait_recv()
    ki = lax.broadcasted_iota(jnp.int32, (256, 256), 0)
    ci = lax.broadcasted_iota(jnp.int32, (256, 256), 1)
    offset = jnp.where(ci < 128, ci, ci - 128) + WINDOW - ki
    band = (offset >= 0) & (offset < WINDOW)
    first = lax.broadcasted_iota(jnp.int32, (1, 256), 1) < 128
    sink = jnp.where(first, sink_ref[0], sink_ref[1])
    for n in range(ROWS // WINDOW):
        lo = n * WINDOW
        q2 = jnp.concatenate([qwin[lo : lo + 128, 0:64], qwin[lo : lo + 128, 64:128]], axis=0)
        kv = ext[lo : lo + 256, :]
        s = contract(kv[:, 0:64], q2, 1, 1) * HEAD ** (-0.5)
        valid = band & (sp * ROWS + lo - WINDOW + ki >= 0)
        s = jnp.where(valid, s, NEGATIVE)
        peak = jnp.maximum(jnp.max(s, axis=0, keepdims=True), sink)
        w = jnp.where(valid, jnp.exp(s - peak), 0.0)
        den = jnp.sum(w, axis=0, keepdims=True) + jnp.exp(sink - peak)
        p = (w / den).astype(BF16)
        o = contract(p, kv[:, 64:128], 0, 0).astype(BF16)
        wout[0, lo : lo + 128, :] = jnp.concatenate([o[:128], o[128:]], axis=1)
    w_cp = [
        remote(wout.at[0], wout.at[d], ws_sem.at[d - 1], wr_sem.at[d - 1], tp_peer(d)) for d in range(1, NTP)
    ]
    for cp in w_cp:
        cp.start()

    m_s[...] = jnp.full((NX, 1, ROWS), NEGATIVE, F32)
    l_s[...] = jnp.zeros((NX, 1, ROWS), F32)
    acc[...] = jnp.zeros((NX, VDIM, ROWS), F32)

    def tile(keys, vals, d, masked):
        s = dot(keys, qbuf[d])
        if masked:
            kpos = lax.broadcasted_iota(jnp.int32, (ROWS, ROWS), 0)
            qpos = lax.broadcasted_iota(jnp.int32, (ROWS, ROWS), 1)
            s = jnp.where(kpos <= qpos, s, NEGATIVE)
        m_old = m_s[d]
        m_new = jnp.maximum(m_old, jnp.max(s, axis=0, keepdims=True))
        p = jnp.exp2((s - m_new) * SOFT)
        alpha = jnp.exp2((m_old - m_new) * SOFT)
        m_s[d] = m_new
        l_s[d] = l_s[d] * alpha + jnp.sum(p, axis=0, keepdims=True)
        acc[d] = acc[d] * alpha + dot(vals, p.astype(BF16))

    def block(slot):
        keys = jnp.concatenate([kbuf[slot], jnp.transpose(rvbuf[slot, 0:64])], axis=1)
        return keys, rvbuf[slot, 64:192]

    def whole(slot):
        keys, vals = block(slot)

        @pl.loop(0, NX)
        def _(d):
            tile(keys, vals, d, False)

    for cp in q_cp:
        cp.wait_recv()
    keys0, vals0 = block(0)
    tile(keys0, vals0, 0, True)

    @pl.loop(1, NX)
    def _(d):
        @pl.when(d > x)
        def _():
            tile(keys0, vals0, d, False)

    for k in range(1, 4):
        k_up[k - 1].wait_recv()
        if k < 3:
            k_up[k].start()
        k_dn[k - 1].wait_recv()
        if k < 3:
            k_dn[k].start()
        else:
            k_far.start()
        v_up[k - 1].wait_recv()
        if k < 3:
            v_up[k].start()
        else:
            v_far.start()
        v_dn[k - 1].wait_recv()
        if k < 3:
            v_dn[k].start()

        @pl.when(z >= k)
        def _():
            whole(k)

        @pl.when(z + k >= NZ)
        def _():
            whole(3 + k)

    k_far.wait_recv()
    v_far.wait_recv()

    @pl.when(z >= 4)
    def _():
        whole(7)

    o_cp = []
    for d in range(1, NX):
        o_send[d - 1] = acc[d].astype(BF16)
        st_send[d - 1, 0:1] = m_s[d]
        st_send[d - 1, 1:2] = l_s[d]
        o_cp.append(remote(o_send.at[d - 1], o_recv.at[d - 1], os_sem.at[d - 1], or_sem.at[d - 1], x_peer(-d)))
        o_cp.append(remote(st_send.at[d - 1], st_recv.at[d - 1], ss_sem.at[d - 1], sr_sem.at[d - 1], x_peer(-d)))
    for cp in o_cp:
        cp.start()

    for cp in branch:
        cp.wait_recv()
    loads[L_BW].wait()
    loads[L_BL].wait()
    for cp in w_cp:
        cp.wait_recv()
    allw = jnp.concatenate([wout[d] for d in range(NTP)], axis=1)
    gatew[...] = gatew[...] * dot(allw, colw[...].reshape(NTP * 128, COLS))

    for cp in o_cp:
        cp.wait_recv()
    ms = [m_s[0]] + [st_recv[d, 0:1] for d in range(3)]
    ls = [l_s[0]] + [st_recv[d, 1:2] for d in range(3)]
    top_m = jnp.maximum(jnp.maximum(ms[0], ms[1]), jnp.maximum(ms[2], ms[3]))
    ws = [jnp.exp2((m - top_m) * SOFT) for m in ms]
    den = ls[0] * ws[0] + ls[1] * ws[1] + ls[2] * ws[2] + ls[3] * ws[3]
    o = acc[0] * ws[0]
    for d in range(3):
        o = o + o_recv[d].astype(F32) * ws[d + 1]
    lat[0] = jnp.transpose(o / den).astype(BF16)
    l_cp = [
        remote(lat.at[0], lat.at[d], ls_sem.at[d - 1], lr_sem.at[d - 1], tp_peer(d)) for d in range(1, NTP)
    ]
    for cp in l_cp:
        cp.start()
    for cp in l_cp:
        cp.wait_recv()
    alll = jnp.concatenate([lat[d] for d in range(NTP)], axis=1)
    out_ref[...] = (gatew[...] + gatel[...] * dot(alll, coll[...].reshape(NTP * 128, COLS))).astype(BF16)

    sent = [f_sib, f_rt, f_rb, f_lb, f_lt, f_ft, f_fb, h_lt, h_lb, h_rb, h_rt, h_ft, h_fb]
    sent += branch + k_up + k_dn + v_up + v_dn + [k_far, v_far] + q_cp + [tail] + w_cp + o_cp + l_cp
    for cp in sent:
        cp.wait_send()


def on_device(
    features, norm_gain, w_query, w_key, w_value, head_sinks, w_query_latent, w_kv_latent, w_rope_key,
    query_latent_gain, kv_latent_gain, w_query_content, w_query_rotary, w_key_up, w_value_up,
    w_branch_window, w_branch_latent, w_gate_window, w_gate_latent,
):
    positions = lax.axis_index("sp") * ROWS + jnp.arange(ROWS, dtype=jnp.int32)
    frequencies = THETA ** (-jnp.arange(ROPE // 2, dtype=F32) / (ROPE // 2))
    angles = frequencies[:, None] * positions.astype(F32)[None, :]
    table = jnp.concatenate([jnp.cos(angles), jnp.sin(angles)], axis=0)
    vmem = pl.BlockSpec(memory_space=pltpu.VMEM)
    anyspace = pl.BlockSpec(memory_space=pl.ANY)
    smem = pl.BlockSpec(memory_space=pltpu.SMEM)
    dma = pltpu.SemaphoreType.DMA
    scratch = [
        pltpu.VMEM((8, ROWS, COLS), BF16),
        pltpu.VMEM((ROWS, D), BF16),
    ]
    weights = [
        w_query, w_key, w_value, w_query_latent, w_kv_latent, w_rope_key, w_query_content, w_query_rotary,
        w_key_up, w_value_up, w_branch_window, w_branch_latent, w_gate_window, w_gate_latent,
    ]
    scratch += [pltpu.VMEM(w.shape, BF16) for w in weights[:10] + weights[12:]]
    scratch += [
        pltpu.VMEM((NTP, 128, COLS), BF16),
        pltpu.VMEM((NTP, 128, COLS), BF16),
        pltpu.VMEM((8, ROWS, NOPE), BF16),
        pltpu.VMEM((8, ROPE + VDIM, ROWS), BF16),
        pltpu.VMEM((NX, NOPE + ROPE, ROWS), BF16),
        pltpu.VMEM((ROWS + WINDOW, 128), BF16),
        pltpu.VMEM((ROWS, 128), BF16),
        pltpu.VMEM((ROWS, COLS), F32),
        pltpu.VMEM((ROWS, COLS), F32),
        pltpu.VMEM((NX, 1, ROWS), F32),
        pltpu.VMEM((NX, 1, ROWS), F32),
        pltpu.VMEM((NX, VDIM, ROWS), F32),
        pltpu.VMEM((NX - 1, VDIM, ROWS), BF16),
        pltpu.VMEM((NX - 1, 2, ROWS), F32),
        pltpu.VMEM((NX - 1, VDIM, ROWS), BF16),
        pltpu.VMEM((NX - 1, 2, ROWS), F32),
        pltpu.VMEM((NTP, ROWS, 128), BF16),
        pltpu.VMEM((NTP, ROWS, 128), BF16),
    ]
    scratch += [
        dma((15,)), dma((13,)), dma((13,)), dma((7,)), dma((7,)), dma((7,)), dma((7,)),
        dma((3,)), dma((3,)), dma(()), dma(()), dma((14,)), dma((14,)),
        dma((3,)), dma((3,)), dma((3,)), dma((3,)), dma((7,)), dma((7,)), dma((7,)), dma((7,)),
    ]
    return pl.pallas_call(
        layer,
        out_shape=jax.ShapeDtypeStruct((ROWS, COLS), BF16),
        in_specs=[anyspace, vmem, vmem, vmem, vmem, smem] + [anyspace] * 14,
        out_specs=vmem,
        scratch_shapes=scratch,
        compiler_params=pltpu.CompilerParams(
            collective_id=0, has_side_effects=True, vmem_limit_bytes=60 * 1024 * 1024
        ),
    )(
        features, norm_gain.reshape(1, D), table, query_latent_gain.reshape(1, LATENT),
        kv_latent_gain.reshape(1, LATENT), head_sinks, *weights,
    )


def solution(mesh):
    return jax.shard_map(
        on_device,
        mesh=mesh,
        in_specs=(
            P("sp", "tp"), P(), P(None, "tp"), P(None, "tp"), P(None, "tp"), P("tp"), P(), P(), P(), P(), P(),
            P(None, "tp"), P(None, "tp"), P(None, "tp"), P(None, "tp"), P("tp", None), P("tp", None),
            P(None, "tp"), P(None, "tp"),
        ),
        out_specs=P("sp", "tp"),
        check_vma=False,
    )
```

time: 252 us -> 81.1 us (0.32); the launches traced: 249 us -> 80.8 us
  waiting for transfers between devices: 125 us -> 0 us
  Pallas kernels: 0 us -> 71.8 us
  matrix products: 54.4 us -> 0 us
  starting transfers between devices: 20.8 us -> 0 us
  other arithmetic: 17.4 us -> 0.92 us
  between operations: 13.9 us -> 0.02 us
  local copies, waits for them, and re-layouts: 17.9 us -> 8.12 us
    all_gather x2 -> x0, waiting for transfers between devices: 85.7 us -> none  [in_one_piece(): result = lax.all_gather(both, axis, axis=dim, tiled=True)]
    pallas_call x0 -> x1, Pallas kernels: none -> 71.8 us  [on_device(): pl.pallas_call(layer, out_shape=jax.ShapeDtypeStruct((ROWS, COLS), BF16),...]
    dot_general x19 -> x0, matrix products: 54.4 us -> none  [the longest x14 17 us: project(): return jnp.dot(left, right, preferred_element_type=jnp.float32)]
    all_to_all x3 -> x0, waiting for transfers between devices: 39 us -> none  [the longest x1 20.7 us: copy_for_each(): lax.all_to_all(jnp.broadcast_to(shard[None], (count, *shard.shape)), axis...]
    all_to_all x3 -> x0, starting transfers between devices: 17.5 us -> none  [the longest x1 7.98 us: on_device(): lax.all_to_all(w_branch_latent, 'tp', split_axis=1, concat_axis=0, tiled=...]
    reduce_sum x3 -> x0, other arithmetic: 13.1 us -> none  [the longest x1 11.1 us: attend(): denominator = jnp.sum(weights, axis=-1)]
    another operation x2 -> x0, local copies, waits for them, and re-layouts: 11.7 us -> none
    unnamed x46 -> x7, local copies, waits for them, and re-layouts: 3.41 us -> 8.12 us
  transfers between devices with their start and end apart: 6 -> 0, of which waited for: 4 -> 0; matrix products, arithmetic and copies ran while one was open for 6% -> 0% of each run, Pallas kernels for 0% -> 0%
where the time goes in v1:
time: 81.1 us; the launch traced here: 80.8 us
  Pallas kernels  71.8 us (89%)
  local copies, waits for them, and re-layouts  8.12 us (10%)
  other arithmetic  0.92 us (1%)
    pallas_call x1, Pallas kernels, on_device(): pl.pallas_call(layer, out_shape=jax.ShapeDtypeStruct((ROWS, COLS), BF16),...  71.8 us
    unnamed x7, local copies, waits for them, and re-layouts  8.12 us

profile of v1, /device:TPU:3, one launch (start us, length us, event | category | flops | bytes accessed | tf_op | source)
XLA Modules:
  0.0 80.8 jit_solution(3526865258429938395)
XLA Ops:
  0.0 0.0 copy-start
  0.0 0.3 multiply_cosine_fusion
  0.3 0.7 pad_maximum_fusion.table_ref
  0.9 1.6 %copy.23.wqr_h = bf16[512,64]{1,0:T(8,128)(2,1)} copy(bf16[512,64]{0,1:T(8,128)(2,1)} %param.31) | data formatting | bytes 131072 | tf_op args[12]
  2.5 1.9 %copy.20.wk_h = bf16[2048,64]{1,0:T(8,128)(2,1)} copy(bf16[2048,64]{0,1:T(8,128)(2,1)} %param.22) | data formatting | bytes 524288 | tf_op args[3]
  4.5 1.9 %copy.21.wv_h = bf16[2048,64]{1,0:T(8,128)(2,1)} copy(bf16[2048,64]{0,1:T(8,128)(2,1)} %param.23) | data formatting | bytes 524288 | tf_op args[4]
  6.4 0.0 copy-done
  6.4 1.0 %copy.22.wr_h = bf16[2048,64]{1,0:T(8,128)(2,1)} copy(bf16[2048,64]{0,1:T(8,128)(2,1)S(1)} %copy-done) | data formatting | bytes 524288 | tf_op args[8]
  7.4 71.8 %shard_map.181 = bf16[384,256]{1,0:T(8,128)(2,1)} custom-call(bf16[384,256]{1,0:T(8,128)(2,1)} %x_ref.1, f32[1,2048]{1,0:T(1,128)} %bitcast.3, f32[64,384]{1,0:T(8,128)} %pad_maximum_fusion.table_ref, f32[1,512]{1,0:T(1,128)} %bitcast.4, f32[1,512]{1,0:T(1,128)} %bitcast.5, f32[2]{0:T(128)} %sink_ref.1, bf16[2048,128]{1,0:T(8,128)(2,1)} %wq_h.1, ...), custom_call_target="tpu_custom_call" | custom-call | tf_op jit(solution)/shard_map/pallas_call | solution.py:431
  79.2 1.6 %copy.25 = bf16[384,256]{1,0:T(8,128)(2,1)} copy(bf16[384,256]{1,0:T(8,128)(2,1)} %shard_map.181) | data formatting | bytes 393216
  (2 shorter events, 0.0 us)
Async XLA Ops:
  0.0 6.4 %copy-start = (bf16[2048,64]{0,1:T(8,128)(2,1)S(1)}, bf16[2048,64]{0,1:T(8,128)(2,1)}, u32[]{:S(2)}) copy-start(bf16[2048,64]{0,1:T(8,128)(2,1)} %param.27) | copy-start | bytes 786436

commit v2 on v1

v2 whole, which is shorter than its diff:
```python
import functools
import math

import jax
import jax.numpy as jnp
from jax import lax
from jax.experimental import pallas as pl
from jax.experimental.pallas import tpu as pltpu
from jax.sharding import PartitionSpec as P

D = 2048
HEAD = 64
WINDOW = 128
NOPE = 128
ROPE = 64
VDIM = 128
LATENT = 512
ROWS = 384
COLS = 256
NX = 4
NY = 4
NZ = 8
NTP = 8
NSP = 32
EPS = 1e-06
THETA = 10000.0
NEGATIVE = -1e30
SOFT = (NOPE + ROPE) ** (-0.5) * math.log2(math.e)
MESH = pl.DeviceIdType.MESH
F32 = jnp.float32
BF16 = jnp.bfloat16


def dot(a, b):
    return jnp.dot(a, b, preferred_element_type=F32)


def contract(a, b, da, db):
    return lax.dot_general(a, b, (((da,), (db,)), ((), ())), preferred_element_type=F32)


def layer(
    x_ref, gain_ref, qgain_ref, kvgain_ref, sink_ref,
    wq_h, wkt_h, wvt_h, wql_h, wkvl_h, wrt_h, wqc_h, wqrt_h, wku_h, wvu_h, wbw_h, wbl_h, wgw_h, wgl_h,
    out_ref,
    feats, normed,
    wq, wrkv, wql, wkvl, wqc, wqrt, wku, wvu, wgw, wgl, trig,
    colw, coll, kbuf, rvbuf, qbuf, ext, qwin, gatew, gatel,
    m_s, l_s, acc, o_send, st_send, o_recv, st_recv, wout, lat,
    w_sem, fs_sem, fr_sem, ks_sem, kr_sem, vs_sem, vr_sem, qs_sem, qr_sem, ts_sem, tr_sem,
    bs_sem, br_sem, os_sem, or_sem, ss_sem, sr_sem, ws_sem, wr_sem, ls_sem, lr_sem,
):
    sp = lax.axis_index("sp")
    tp = lax.axis_index("tp")
    z = sp // NX
    x = sp % NX
    y = tp // 2
    c = tp % 2

    def z_peer(by):
        return (((z + by + NZ) % NZ) * NX + x, tp)

    def x_peer(by):
        return (z * NX + (x + by + NX) % NX, tp)

    def y_peer(by):
        return (sp, ((y + by + NY) % NY) * 2 + c)

    def tp_peer(by):
        return (sp, (tp + by + NTP) % NTP)

    def sp_peer(by):
        return ((sp + by + NSP) % NSP, tp)

    sibling = (sp, tp + 1 - 2 * c)

    def remote(src, dst, ssem, rsem, dev):
        return pltpu.make_async_remote_copy(
            src_ref=src, dst_ref=dst, send_sem=ssem, recv_sem=rsem, device_id=dev, device_id_type=MESH
        )

    own_cols = pl.ds(pl.multiple_of(tp * COLS, COLS), COLS)
    pairs = [
        (wkvl_h, wkvl), (wrt_h, wrkv.at[pl.ds(0, 64)]), (wku_h, wku), (wvu_h, wvu), (wql_h, wql), (wqc_h, wqc),
        (wqrt_h, wqrt), (wq_h, wq), (wkt_h, wrkv.at[pl.ds(64, 64)]), (wvt_h, wrkv.at[pl.ds(128, 64)]),
        (wgw_h, wgw), (wgl_h, wgl),
        (wbw_h.at[:, own_cols], colw.at[0]), (wbl_h.at[:, own_cols], coll.at[0]),
        (x_ref, feats.at[0]),
    ]
    loads = [pltpu.make_async_copy(a, b, w_sem.at[i]) for i, (a, b) in enumerate(pairs)]
    (L_KVL, L_R, L_KU, L_VU, L_QL, L_QC, L_QR, L_Q, L_K, L_V, L_GW, L_GL, L_BW, L_BL, L_X) = range(15)
    loads[L_X].start()
    for i in range(14):
        loads[i].start()

    barrier = pltpu.get_barrier_semaphore()
    partners = [z_peer(1), z_peer(-1), sp_peer(1), sp_peer(-1)]
    partners += [x_peer(d) for d in range(1, NX)]
    partners += [tp_peer(d) for d in range(1, NTP)]
    for dev in partners:
        pl.semaphore_signal(barrier, inc=1, device_id=dev, device_id_type=MESH)
    spots = lax.broadcasted_iota(jnp.int32, (ROPE // 2, ROWS), 1) + sp * ROWS
    freq_at = lax.broadcasted_iota(jnp.int32, (ROPE // 2, ROWS), 0)
    frequencies = jnp.exp(freq_at.astype(F32) * (-math.log(THETA) / (ROPE // 2)))
    angles = spots.astype(F32) * frequencies
    trig[0:32, :] = jnp.cos(angles)
    trig[32:64, :] = jnp.sin(angles)
    pl.semaphore_wait(barrier, len(partners))
    loads[L_X].wait()

    half = ROWS // 2
    top, bot = pl.ds(0, half), pl.ds(half, half)

    def spread(buf, ssem, rsem):
        def part(i, src, dst, rows, dev):
            return remote(buf.at[src, rows], buf.at[dst, rows], ssem.at[i], rsem.at[i], dev)

        return dict(
            sib=remote(buf.at[0], buf.at[1], ssem.at[0], rsem.at[0], sibling),
            rt=part(1, 0, 2, top, y_peer(1)),
            rb=part(2, 0, 2, bot, y_peer(1)),
            lb=part(3, 0, 6, bot, y_peer(-1)),
            lt=part(4, 0, 6, top, y_peer(-1)),
            ft=part(5, 2, 4, top, y_peer(1)),
            fb=part(6, 6, 4, bot, y_peer(-1)),
            hlt=part(7, 2, 3, top, sibling),
            hlb=part(8, 2, 3, bot, sibling),
            hrb=part(9, 6, 7, bot, sibling),
            hrt=part(10, 6, 7, top, sibling),
            hft=part(11, 4, 5, top, sibling),
            hfb=part(12, 4, 5, bot, sibling),
        )

    def spread_first(cp):
        for name in ("rt", "lb", "rb", "lt", "sib"):
            cp[name].start()

    def spread_second(cp):
        for name, fwd, hand in (("rt", "ft", "hlt"), ("lb", "fb", "hrb"), ("rb", None, "hlb"), ("lt", None, "hrt")):
            cp[name].wait_recv()
            if fwd:
                cp[fwd].start()
            cp[hand].start()

    def spread_third(cp):
        for name, hand in (("ft", "hft"), ("fb", "hfb")):
            cp[name].wait_recv()
            cp[hand].start()

    f_cp = spread(feats, fs_sem, fr_sem)
    spread_first(f_cp)
    spread_second(f_cp)

    def squares(i):
        v = feats[i].astype(F32)
        v = v * v
        return v[:, :128] + v[:, 128:]

    f_cp["sib"].wait_recv()
    total = squares(0) + squares(1) + squares(2) + squares(6)
    for name in ("hlt", "hlb", "hrb", "hrt"):
        f_cp[name].wait_recv()
    total = total + squares(3) + squares(7)
    spread_third(f_cp)
    total = total + squares(4)
    for name in ("hft", "hfb"):
        f_cp[name].wait_recv()
    total = total + squares(5)
    inv = lax.rsqrt(jnp.sum(total, axis=-1, keepdims=True) * (1.0 / D) + EPS)

    for i in range(8):
        dy, dc = i // 2, i % 2
        src = ((y - dy + NY) % NY) * 2 + (c if dc == 0 else 1 - c)
        cols = pl.ds(pl.multiple_of(src * COLS, COLS), COLS)
        normed[:, cols] = (feats[i].astype(F32) * inv * gain_ref[:, cols]).astype(BF16)

    def rms(v, g):
        return (v * lax.rsqrt(jnp.mean(v * v, axis=-1, keepdims=True) + EPS) * g[...]).astype(BF16)

    cos_t = trig[0:32, :]
    sin_t = trig[32:64, :]

    def rotate_t(v):
        a, b = v[:32], v[32:]
        return jnp.concatenate([a * cos_t - b * sin_t, b * cos_t + a * sin_t], axis=0)

    loads[L_KVL].wait()
    loads[L_R].wait()
    loads[L_KU].wait()
    loads[L_VU].wait()
    loads[L_K].wait()
    loads[L_V].wait()
    lkv = rms(dot(normed[...], wkvl[...]), kvgain_ref)
    kbuf[0] = dot(lkv, wku[...]).astype(BF16)
    rvbuf[0, 64:192] = jnp.transpose(dot(lkv, wvu[...])).astype(BF16)
    rkv = contract(normed[...], wrkv[...], 1, 1)
    rvbuf[0, 0:64] = rotate_t(jnp.transpose(rkv[:, 0:64])).astype(BF16)
    ext[WINDOW:, :] = rkv[:, 64:192].astype(BF16)

    def k_copy(i, src, dst, dev):
        return remote(kbuf.at[src], kbuf.at[dst], ks_sem.at[i], kr_sem.at[i], dev)

    def v_copy(i, src, dst, dev):
        return remote(rvbuf.at[src], rvbuf.at[dst], vs_sem.at[i], vr_sem.at[i], dev)

    up, down = z_peer(1), z_peer(-1)
    ups = [(0, 0, 1), (1, 1, 2), (2, 2, 3)]
    downs = [(3, 0, 4), (4, 4, 5), (5, 5, 6)]
    k_up = [k_copy(*t, up) for t in ups]
    v_up = [v_copy(*t, up) for t in ups]
    k_dn = [k_copy(*t, down) for t in downs]
    v_dn = [v_copy(*t, down) for t in downs]
    k_far = k_copy(6, 6, 7, down)
    v_far = v_copy(6, 3, 7, up)
    k_up[0].start()
    k_dn[0].start()
    v_up[0].start()
    v_dn[0].start()

    tail = remote(ext.at[pl.ds(ROWS, WINDOW)], ext.at[pl.ds(0, WINDOW)], ts_sem, tr_sem, sp_peer(1))
    tail.start()

    loads[L_QL].wait()
    loads[L_QC].wait()
    loads[L_QR].wait()
    lq = rms(dot(normed[...], wql[...]), qgain_ref)
    qbuf[0:128, 0:ROWS] = jnp.transpose(dot(lq, wqc[...])).astype(BF16)
    qbuf[128:192, 0:ROWS] = rotate_t(contract(wqrt[...], lq, 1, 1)).astype(BF16)
    slots = [pl.ds(d * ROWS, ROWS) for d in range(NX)]
    q_half = (pl.ds(0, 96), pl.ds(96, 96))

    def q_copy(i, rows, src, dst, by):
        return remote(
            qbuf.at[rows, slots[src]], qbuf.at[rows, slots[dst]], qs_sem.at[i], qr_sem.at[i], x_peer(by)
        )

    q_all = pl.ds(0, NOPE + ROPE)
    q_cp = [q_copy(0, q_all, 0, 1, 1), q_copy(1, q_all, 0, 3, -1)]
    q_fwd = [q_copy(2, q_half[0], 1, 2, 1), q_copy(3, q_half[1], 3, 2, -1)]
    for cp in q_cp:
        cp.start()

    branch = []
    for slot in range(1, NTP):
        dy, dc = slot // 2, slot % 2
        peer = ((y + dy) % NY) * 2 + (c if dc == 0 else 1 - c)
        cols = pl.ds(pl.multiple_of(peer * COLS, COLS), COLS)
        i, j = slot - 1, slot + 6
        branch.append(remote(wbw_h.at[:, cols], colw.at[slot], bs_sem.at[i], br_sem.at[i], (sp, peer)))
        branch.append(remote(wbl_h.at[:, cols], coll.at[slot], bs_sem.at[j], br_sem.at[j], (sp, peer)))
    for cp in branch:
        cp.start()

    loads[L_Q].wait()
    qwin[...] = dot(normed[...], wq[...]).astype(BF16)
    loads[L_GW].wait()
    loads[L_GL].wait()
    gatew[...] = jax.nn.sigmoid(dot(normed[...], wgw[...]))
    gatel[...] = jax.nn.sigmoid(dot(normed[...], wgl[...]))

    def windowed():
        tail.wait_recv()
        ki = lax.broadcasted_iota(jnp.int32, (256, 256), 0)
        ci = lax.broadcasted_iota(jnp.int32, (256, 256), 1)
        offset = jnp.where(ci < 128, ci, ci - 128) + WINDOW - ki
        band = (offset >= 0) & (offset < WINDOW)
        first = lax.broadcasted_iota(jnp.int32, (1, 256), 1) < 128
        sink = jnp.where(first, sink_ref[0], sink_ref[1])
        for n in range(ROWS // WINDOW):
            lo = n * WINDOW
            q2 = jnp.concatenate([qwin[lo : lo + 128, 0:64], qwin[lo : lo + 128, 64:128]], axis=0)
            kv = ext[lo : lo + 256, :]
            s = contract(kv[:, 0:64], q2, 1, 1) * HEAD ** (-0.5)
            valid = band & (sp * ROWS + lo - WINDOW + ki >= 0)
            s = jnp.where(valid, s, NEGATIVE)
            peak = jnp.maximum(jnp.max(s, axis=0, keepdims=True), sink)
            w = jnp.where(valid, jnp.exp(s - peak), 0.0)
            den = jnp.sum(w, axis=0, keepdims=True) + jnp.exp(sink - peak)
            p = (w / den).astype(BF16)
            o = contract(p, kv[:, 64:128], 0, 0).astype(BF16)
            wout[0, lo : lo + 128, :] = jnp.concatenate([o[:128], o[128:]], axis=1)
        spread_first(w_cp)

    w_cp = spread(wout, ws_sem, wr_sem)

    m_s[...] = jnp.full((1, NX * ROWS), NEGATIVE, F32)
    l_s[...] = jnp.zeros((1, NX * ROWS), F32)
    acc[...] = jnp.zeros((VDIM, NX * ROWS), F32)

    def tile(keys, vals, cols, masked):
        s = dot(keys, qbuf[:, cols])
        if masked:
            kpos = lax.broadcasted_iota(jnp.int32, (ROWS, ROWS), 0)
            qpos = lax.broadcasted_iota(jnp.int32, (ROWS, ROWS), 1)
            s = jnp.where(kpos <= qpos, s, NEGATIVE)
        m_old = m_s[:, cols]
        m_new = jnp.maximum(m_old, jnp.max(s, axis=0, keepdims=True))
        p = jnp.exp2((s - m_new) * SOFT)
        alpha = jnp.exp2((m_old - m_new) * SOFT)
        m_s[:, cols] = m_new
        l_s[:, cols] = l_s[:, cols] * alpha + jnp.sum(p, axis=0, keepdims=True)
        acc[:, cols] = acc[:, cols] * alpha + dot(vals, p.astype(BF16))

    def block(slot):
        keys = jnp.concatenate([kbuf[slot], jnp.transpose(rvbuf[slot, 0:64])], axis=1)
        return keys, rvbuf[slot, 64:192]

    def whole(slot, useful):
        @pl.when(useful)
        def _():
            keys, vals = block(slot)
            tile(keys, vals, pl.ds(0, NX * ROWS), False)

    def own():
        keys, vals = block(0)
        tile(keys, vals, slots[0], True)
        for d in range(1, NX):

            @pl.when(d > x)
            def _():
                tile(keys, vals, slots[d], False)

    def relay(arrived, after):
        for cp, nxt in zip(arrived, after):
            cp.wait_recv()
            if nxt is not None:
                nxt.start()

    relay((k_up[0], k_dn[0]), (k_up[1], k_dn[1]))
    relay((v_up[0], v_dn[0]), (v_up[1], v_dn[1]))
    relay(q_cp, q_fwd)
    windowed()
    relay((k_up[1], k_dn[1]), (k_up[2], k_dn[2]))
    relay(q_fwd, (None, None))
    own()
    relay((v_up[1], v_dn[1]), (v_up[2], v_dn[2]))
    whole(1, z >= 1)
    relay((k_up[2], k_dn[2]), (None, k_far))
    whole(4, z >= 7)
    spread_second(w_cp)
    relay((v_up[2], v_dn[2]), (v_far, None))
    whole(2, z >= 2)
    whole(5, z >= 6)
    spread_third(w_cp)
    whole(3, z >= 3)
    whole(6, z >= 5)
    relay((k_far, v_far), (None, None))
    whole(7, z >= 4)

    o_cp = []
    for d in range(1, NX):
        o_send[d - 1] = acc[:, slots[d]].astype(BF16)
        st_send[d - 1, 0:1] = m_s[:, slots[d]]
        st_send[d - 1, 1:2] = l_s[:, slots[d]]
        o_cp.append(remote(o_send.at[d - 1], o_recv.at[d - 1], os_sem.at[d - 1], or_sem.at[d - 1], x_peer(-d)))
        o_cp.append(remote(st_send.at[d - 1], st_recv.at[d - 1], ss_sem.at[d - 1], sr_sem.at[d - 1], x_peer(-d)))
    for cp in o_cp:
        cp.start()

    for cp in branch:
        cp.wait_recv()
    loads[L_BW].wait()
    loads[L_BL].wait()
    for name in ("sib", "hlt", "hlb", "hrb", "hrt", "hft", "hfb"):
        w_cp[name].wait_recv()
    allw = jnp.concatenate([wout[d] for d in range(NTP)], axis=1)
    gatew[...] = gatew[...] * dot(allw, colw[...].reshape(NTP * 128, COLS))

    for cp in o_cp:
        cp.wait_recv()
    ms = [m_s[:, slots[0]]] + [st_recv[d, 0:1] for d in range(3)]
    ls = [l_s[:, slots[0]]] + [st_recv[d, 1:2] for d in range(3)]
    top_m = jnp.maximum(jnp.maximum(ms[0], ms[1]), jnp.maximum(ms[2], ms[3]))
    ws = [jnp.exp2((m - top_m) * SOFT) for m in ms]
    den = ls[0] * ws[0] + ls[1] * ws[1] + ls[2] * ws[2] + ls[3] * ws[3]
    o = acc[:, slots[0]] * ws[0]
    for d in range(3):
        o = o + o_recv[d].astype(F32) * ws[d + 1]
    lat[0] = jnp.transpose(o / den).astype(BF16)
    l_cp = spread(lat, ls_sem, lr_sem)
    spread_first(l_cp)
    spread_second(l_cp)
    l_cp["sib"].wait_recv()

    def branch_part(first, count):
        rows = jnp.concatenate([lat[i] for i in range(first, first + count)], axis=1)
        return dot(rows, coll[first : first + count].reshape(count * 128, COLS))

    mixed = branch_part(0, 2)
    spread_third(l_cp)
    for name in ("hlt", "hlb", "hrb", "hrt"):
        l_cp[name].wait_recv()
    mixed = mixed + branch_part(2, 2) + branch_part(6, 2)
    for name in ("hft", "hfb"):
        l_cp[name].wait_recv()
    mixed = mixed + branch_part(4, 2)
    out_ref[...] = (gatew[...] + gatel[...] * mixed).astype(BF16)

    sent = list(f_cp.values()) + list(w_cp.values()) + list(l_cp.values())
    sent += branch + k_up + k_dn + v_up + v_dn + [k_far, v_far] + q_cp + q_fwd + [tail] + o_cp
    for cp in sent:
        cp.wait_send()


def on_device(
    features, norm_gain, w_query, w_key, w_value, head_sinks, w_query_latent, w_kv_latent, w_rope_key,
    query_latent_gain, kv_latent_gain, w_query_content, w_query_rotary, w_key_up, w_value_up,
    w_branch_window, w_branch_latent, w_gate_window, w_gate_latent,
):
    vmem = pl.BlockSpec(memory_space=pltpu.VMEM)
    anyspace = pl.BlockSpec(memory_space=pl.ANY)
    smem = pl.BlockSpec(memory_space=pltpu.SMEM)
    dma = pltpu.SemaphoreType.DMA
    scratch = [
        pltpu.VMEM((8, ROWS, COLS), BF16),
        pltpu.VMEM((ROWS, D), BF16),
    ]
    weights = [
        w_query, w_key.T, w_value.T, w_query_latent, w_kv_latent, w_rope_key.T, w_query_content, w_query_rotary.T,
        w_key_up, w_value_up, w_branch_window, w_branch_latent, w_gate_window, w_gate_latent,
    ]
    shapes = [
        (D, 128), (192, D), (D, LATENT), (D, LATENT), (LATENT, NOPE), (ROPE, LATENT), (LATENT, NOPE), (LATENT, VDIM),
        (D, COLS), (D, COLS),
    ]
    scratch += [pltpu.VMEM(shape, BF16) for shape in shapes] + [pltpu.VMEM((ROPE, ROWS), F32)]
    scratch += [
        pltpu.VMEM((NTP, 128, COLS), BF16),
        pltpu.VMEM((NTP, 128, COLS), BF16),
        pltpu.VMEM((8, ROWS, NOPE), BF16),
        pltpu.VMEM((8, ROPE + VDIM, ROWS), BF16),
        pltpu.VMEM((NOPE + ROPE, NX * ROWS), BF16),
        pltpu.VMEM((ROWS + WINDOW, 128), BF16),
        pltpu.VMEM((ROWS, 128), BF16),
        pltpu.VMEM((ROWS, COLS), F32),
        pltpu.VMEM((ROWS, COLS), F32),
        pltpu.VMEM((1, NX * ROWS), F32),
        pltpu.VMEM((1, NX * ROWS), F32),
        pltpu.VMEM((VDIM, NX * ROWS), F32),
        pltpu.VMEM((NX - 1, VDIM, ROWS), BF16),
        pltpu.VMEM((NX - 1, 2, ROWS), F32),
        pltpu.VMEM((NX - 1, VDIM, ROWS), BF16),
        pltpu.VMEM((NX - 1, 2, ROWS), F32),
        pltpu.VMEM((NTP, ROWS, 128), BF16),
        pltpu.VMEM((NTP, ROWS, 128), BF16),
    ]
    scratch += [
        dma((15,)), dma((13,)), dma((13,)), dma((7,)), dma((7,)), dma((7,)), dma((7,)),
        dma((4,)), dma((4,)), dma(()), dma(()), dma((14,)), dma((14,)),
        dma((3,)), dma((3,)), dma((3,)), dma((3,)), dma((13,)), dma((13,)), dma((13,)), dma((13,)),
    ]
    return pl.pallas_call(
        layer,
        out_shape=pltpu.VMEM((ROWS, COLS), BF16),
        in_specs=[anyspace, vmem, vmem, vmem, smem] + [anyspace] * 14,
        out_specs=vmem,
        scratch_shapes=scratch,
        compiler_params=pltpu.CompilerParams(
            collective_id=0, has_side_effects=True, vmem_limit_bytes=60 * 1024 * 1024
        ),
    )(
        features, norm_gain.reshape(1, D), query_latent_gain.reshape(1, LATENT),
        kv_latent_gain.reshape(1, LATENT), head_sinks, *weights,
    )


def solution(mesh):
    return jax.shard_map(
        on_device,
        mesh=mesh,
        in_specs=(
            P("sp", "tp"), P(), P(None, "tp"), P(None, "tp"), P(None, "tp"), P("tp"), P(), P(), P(), P(), P(),
            P(None, "tp"), P(None, "tp"), P(None, "tp"), P(None, "tp"), P("tp", None), P("tp", None),
            P(None, "tp"), P(None, "tp"),
        ),
        out_specs=P("sp", "tp"),
        check_vma=False,
    )
```

time: 81.1 us -> 64.4 us (0.79)
  Pallas kernels: 71.8 us -> 62.8 us
  local copies, waits for them, and re-layouts: 8.12 us -> 0.68 us
  other arithmetic: 0.92 us -> 0 us
    pallas_call x1, Pallas kernels: 71.8 us -> 62.8 us  [on_device(): pl.pallas_call(layer, out_shape=pltpu.VMEM((ROWS, COLS), BF16), in_specs=...]
    unnamed x7 -> x1, local copies, waits for them, and re-layouts: 8.12 us -> 0.68 us
where the time goes in v2:
time: 64.4 us; the launch traced here: 63.5 us
  Pallas kernels  62.8 us (98%)
  local copies, waits for them, and re-layouts  0.68 us (1%)
    pallas_call x1, Pallas kernels, on_device(): pl.pallas_call(layer, out_shape=pltpu.VMEM((ROWS, COLS), BF16), in_specs=...  62.8 us

profile of v2, /device:TPU:3, one launch (start us, length us, event | category | flops | bytes accessed | tf_op | source)
XLA Modules:
  0.0 63.5 jit_solution(16498154829592860736)
XLA Ops:
  0.0 62.8 %shard_map.181 = bf16[384,256]{1,0:T(8,128)(2,1)S(1)} custom-call(bf16[384,256]{1,0:T(8,128)(2,1)} %x_ref.1, f32[1,2048]{1,0:T(1,128)} %bitcast.11, f32[1,512]{1,0:T(1,128)} %bitcast.12, f32[1,512]{1,0:T(1,128)} %bitcast.13, f32[2]{0:T(128)} %sink_ref.1, bf16[2048,128]{1,0:T(8,128)(2,1)} %wq_h.1, bf16[64,2048]{1,0:T(8,128)(2,1)} %bitcast.7, ...), custom_call_target="tpu_custom_call" | custom-call | tf_op jit(solution)/shard_map/pallas_call | solution.py:452
  62.8 0.7 %copy.21 = bf16[384,256]{1,0:T(8,128)(2,1)} copy(bf16[384,256]{1,0:T(8,128)(2,1)S(1)} %shard_map.181) | data formatting | bytes 393216

commit v3 on v2

--- a/solution.py
+++ b/solution.py
@@ -108,15 +108,15 @@
     pl.semaphore_wait(barrier, len(partners))
     loads[L_X].wait()
 
-    half = ROWS // 2
-    top, bot = pl.ds(0, half), pl.ds(half, half)
-
-    def spread(buf, ssem, rsem):
+    def spread(buf, ssem, rsem, lo=0, count=ROWS, first=0):
+        half = count // 2
+        every, top, bot = pl.ds(lo, count), pl.ds(lo, half), pl.ds(lo + half, half)
+
         def part(i, src, dst, rows, dev):
-            return remote(buf.at[src, rows], buf.at[dst, rows], ssem.at[i], rsem.at[i], dev)
+            return remote(buf.at[src, rows], buf.at[dst, rows], ssem.at[first + i], rsem.at[first + i], dev)
 
         return dict(
-            sib=remote(buf.at[0], buf.at[1], ssem.at[0], rsem.at[0], sibling),
+            sib=part(0, 0, 1, every, sibling),
             rt=part(1, 0, 2, top, y_peer(1)),
             rb=part(2, 0, 2, bot, y_peer(1)),
             lb=part(3, 0, 6, bot, y_peer(-1)),
@@ -212,10 +212,38 @@
     v_dn = [v_copy(*t, down) for t in downs]
     k_far = k_copy(6, 6, 7, down)
     v_far = v_copy(6, 3, 7, up)
-    k_up[0].start()
-    k_dn[0].start()
-    v_up[0].start()
-    v_dn[0].start()
+
+    def up_got(k):
+        return z >= k
+
+    def up_go(k):
+        return (z >= k) & (z < NZ - 1)
+
+    def k_down(k):
+        return (z + k) % NZ <= 3
+
+    def v_down(k):
+        return (z + k) % NZ <= 2
+
+    def when_start(cond, cp):
+        @pl.when(cond)
+        def _():
+            cp.start()
+
+    def when_recv(cond, cp):
+        @pl.when(cond)
+        def _():
+            cp.wait_recv()
+
+    def when_sent(cond, cp):
+        @pl.when(cond)
+        def _():
+            cp.wait_send()
+
+    when_start(up_go(0), k_up[0])
+    when_start(k_down(0), k_dn[0])
+    when_start(up_go(0), v_up[0])
+    when_start(v_down(0), v_dn[0])
 
     tail = remote(ext.at[pl.ds(ROWS, WINDOW)], ext.at[pl.ds(0, WINDOW)], ts_sem, tr_sem, sp_peer(1))
     tail.start()
@@ -320,42 +348,59 @@
             def _():
                 tile(keys, vals, slots[d], False)
 
-    def relay(arrived, after):
-        for cp, nxt in zip(arrived, after):
-            cp.wait_recv()
-            if nxt is not None:
-                nxt.start()
-
-    relay((k_up[0], k_dn[0]), (k_up[1], k_dn[1]))
-    relay((v_up[0], v_dn[0]), (v_up[1], v_dn[1]))
-    relay(q_cp, q_fwd)
+    def relay_k(k):
+        when_recv(up_got(k), k_up[k - 1])
+        if k < 3:
+            when_start(up_go(k), k_up[k])
+        when_recv(k_down(k), k_dn[k - 1])
+        when_start(k_down(k), k_dn[k] if k < 3 else k_far)
+
+    def relay_v(k):
+        when_recv(up_got(k), v_up[k - 1])
+        when_start(up_go(k), v_up[k] if k < 3 else v_far)
+        when_recv(v_down(k), v_dn[k - 1])
+        if k < 3:
+            when_start(v_down(k), v_dn[k])
+
+    relay_k(1)
+    relay_v(1)
+    for cp, nxt in zip(q_cp, q_fwd):
+        cp.wait_recv()
+        nxt.start()
     windowed()
-    relay((k_up[1], k_dn[1]), (k_up[2], k_dn[2]))
-    relay(q_fwd, (None, None))
+    relay_k(2)
+    for cp in q_fwd:
+        cp.wait_recv()
     own()
-    relay((v_up[1], v_dn[1]), (v_up[2], v_dn[2]))
+    relay_v(2)
     whole(1, z >= 1)
-    relay((k_up[2], k_dn[2]), (None, k_far))
+    relay_k(3)
     whole(4, z >= 7)
     spread_second(w_cp)
-    relay((v_up[2], v_dn[2]), (v_far, None))
+    relay_v(3)
     whole(2, z >= 2)
     whole(5, z >= 6)
     spread_third(w_cp)
     whole(3, z >= 3)
     whole(6, z >= 5)
-    relay((k_far, v_far), (None, None))
+    when_recv(z >= 4, k_far)
+    when_recv(z >= 4, v_far)
     whole(7, z >= 4)
 
-    o_cp = []
-    for d in range(1, NX):
-        o_send[d - 1] = acc[:, slots[d]].astype(BF16)
+    pieces = [pl.ds(p * 128, 128) for p in range(3)]
+    st_cp, o_cp = [], [[], [], []]
+    for d in (2, 1, 3):
         st_send[d - 1, 0:1] = m_s[:, slots[d]]
         st_send[d - 1, 1:2] = l_s[:, slots[d]]
-        o_cp.append(remote(o_send.at[d - 1], o_recv.at[d - 1], os_sem.at[d - 1], or_sem.at[d - 1], x_peer(-d)))
-        o_cp.append(remote(st_send.at[d - 1], st_recv.at[d - 1], ss_sem.at[d - 1], sr_sem.at[d - 1], x_peer(-d)))
-    for cp in o_cp:
+        st_cp.append(remote(st_send.at[d - 1], st_recv.at[d - 1], ss_sem.at[d - 1], sr_sem.at[d - 1], x_peer(-d)))
+    for cp in st_cp:
         cp.start()
+    for p in range(3):
+        for d in (2, 1, 3):
+            i = (d - 1) * 3 + p
+            o_send[i] = acc[:, pl.ds(d * ROWS + p * 128, 128)].astype(BF16)
+            o_cp[p].append(remote(o_send.at[i], o_recv.at[i], os_sem.at[i], or_sem.at[i], x_peer(-d)))
+            o_cp[p][-1].start()
 
     for cp in branch:
         cp.wait_recv()
@@ -366,38 +411,54 @@
     allw = jnp.concatenate([wout[d] for d in range(NTP)], axis=1)
     gatew[...] = gatew[...] * dot(allw, colw[...].reshape(NTP * 128, COLS))
 
-    for cp in o_cp:
+    l_cp = [spread(lat, ls_sem, lr_sem, p * 128, 128, p * 13) for p in range(3)]
+    for cp in st_cp:
         cp.wait_recv()
-    ms = [m_s[:, slots[0]]] + [st_recv[d, 0:1] for d in range(3)]
-    ls = [l_s[:, slots[0]]] + [st_recv[d, 1:2] for d in range(3)]
-    top_m = jnp.maximum(jnp.maximum(ms[0], ms[1]), jnp.maximum(ms[2], ms[3]))
-    ws = [jnp.exp2((m - top_m) * SOFT) for m in ms]
-    den = ls[0] * ws[0] + ls[1] * ws[1] + ls[2] * ws[2] + ls[3] * ws[3]
-    o = acc[:, slots[0]] * ws[0]
-    for d in range(3):
-        o = o + o_recv[d].astype(F32) * ws[d + 1]
-    lat[0] = jnp.transpose(o / den).astype(BF16)
-    l_cp = spread(lat, ls_sem, lr_sem)
-    spread_first(l_cp)
-    spread_second(l_cp)
-    l_cp["sib"].wait_recv()
+    for p, cols in enumerate(pieces):
+        for cp in o_cp[p]:
+            cp.wait_recv()
+        ms = [m_s[:, cols]] + [st_recv[d, 0:1, cols] for d in range(3)]
+        ls = [l_s[:, cols]] + [st_recv[d, 1:2, cols] for d in range(3)]
+        top_m = jnp.maximum(jnp.maximum(ms[0], ms[1]), jnp.maximum(ms[2], ms[3]))
+        ws = [jnp.exp2((m - top_m) * SOFT) for m in ms]
+        den = ls[0] * ws[0] + ls[1] * ws[1] + ls[2] * ws[2] + ls[3] * ws[3]
+        o = acc[:, cols] * ws[0]
+        for d in range(3):
+            o = o + o_recv[d * 3 + p].astype(F32) * ws[d + 1]
+        lat[0, cols] = jnp.transpose(o / den).astype(BF16)
+        spread_first(l_cp[p])
+    for cp in l_cp:
+        spread_second(cp)
+    for cp in l_cp:
+        cp["sib"].wait_recv()
 
     def branch_part(first, count):
         rows = jnp.concatenate([lat[i] for i in range(first, first + count)], axis=1)
         return dot(rows, coll[first : first + count].reshape(count * 128, COLS))
 
     mixed = branch_part(0, 2)
-    spread_third(l_cp)
-    for name in ("hlt", "hlb", "hrb", "hrt"):
-        l_cp[name].wait_recv()
+    for cp in l_cp:
+        spread_third(cp)
+    for cp in l_cp:
+        for name in ("hlt", "hlb", "hrb", "hrt"):
+            cp[name].wait_recv()
     mixed = mixed + branch_part(2, 2) + branch_part(6, 2)
-    for name in ("hft", "hfb"):
-        l_cp[name].wait_recv()
+    for cp in l_cp:
+        for name in ("hft", "hfb"):
+            cp[name].wait_recv()
     mixed = mixed + branch_part(4, 2)
     out_ref[...] = (gatew[...] + gatel[...] * mixed).astype(BF16)
 
-    sent = list(f_cp.values()) + list(w_cp.values()) + list(l_cp.values())
-    sent += branch + k_up + k_dn + v_up + v_dn + [k_far, v_far] + q_cp + q_fwd + [tail] + o_cp
+    sent = list(f_cp.values()) + list(w_cp.values()) + branch + q_cp + q_fwd + [tail] + st_cp
+    for p in range(3):
+        sent += list(l_cp[p].values()) + o_cp[p]
+    for k in range(3):
+        when_sent(up_go(k), k_up[k])
+        when_sent(up_go(k), v_up[k])
+        when_sent(k_down(k), k_dn[k])
+        when_sent(v_down(k), v_dn[k])
+    when_sent(k_down(3), k_far)
+    when_sent(up_go(3), v_far)
     for cp in sent:
         cp.wait_send()
 
@@ -437,9 +498,9 @@
         pltpu.VMEM((1, NX * ROWS), F32),
         pltpu.VMEM((1, NX * ROWS), F32),
         pltpu.VMEM((VDIM, NX * ROWS), F32),
-        pltpu.VMEM((NX - 1, VDIM, ROWS), BF16),
+        pltpu.VMEM((9, VDIM, 128), BF16),
         pltpu.VMEM((NX - 1, 2, ROWS), F32),
-        pltpu.VMEM((NX - 1, VDIM, ROWS), BF16),
+        pltpu.VMEM((9, VDIM, 128), BF16),
         pltpu.VMEM((NX - 1, 2, ROWS), F32),
         pltpu.VMEM((NTP, ROWS, 128), BF16),
         pltpu.VMEM((NTP, ROWS, 128), BF16),
@@ -447,7 +508,7 @@
     scratch += [
         dma((15,)), dma((13,)), dma((13,)), dma((7,)), dma((7,)), dma((7,)), dma((7,)),
         dma((4,)), dma((4,)), dma(()), dma(()), dma((14,)), dma((14,)),
-        dma((3,)), dma((3,)), dma((3,)), dma((3,)), dma((13,)), dma((13,)), dma((13,)), dma((13,)),
+        dma((9,)), dma((9,)), dma((3,)), dma((3,)), dma((13,)), dma((13,)), dma((39,)), dma((39,)),
     ]
     return pl.pallas_call(
         layer,

time: 64.4 us -> 60.1 us (0.933)
  Pallas kernels: 62.8 us -> 58.2 us
    pallas_call x1, Pallas kernels: 62.8 us -> 58.2 us  [on_device(): pl.pallas_call(layer, out_shape=pltpu.VMEM((ROWS, COLS), BF16), in_specs=...]
where the time goes in v3:
time: 60.1 us; the launch traced here: 58.9 us
  Pallas kernels  58.2 us (97%)
  local copies, waits for them, and re-layouts  0.68 us (1%)
    pallas_call x1, Pallas kernels, on_device(): pl.pallas_call(layer, out_shape=pltpu.VMEM((ROWS, COLS), BF16), in_specs=...  58.2 us

profile of v3, /device:TPU:3, one launch (start us, length us, event | category | flops | bytes accessed | tf_op | source)
XLA Modules:
  0.0 58.9 jit_solution(10140488192967213270)
XLA Ops:
  0.0 58.2 %shard_map.181 = bf16[384,256]{1,0:T(8,128)(2,1)S(1)} custom-call(bf16[384,256]{1,0:T(8,128)(2,1)} %x_ref.1, f32[1,2048]{1,0:T(1,128)} %bitcast.11, f32[1,512]{1,0:T(1,128)} %bitcast.12, f32[1,512]{1,0:T(1,128)} %bitcast.13, f32[2]{0:T(128)} %sink_ref.1, bf16[2048,128]{1,0:T(8,128)(2,1)} %wq_h.1, bf16[64,2048]{1,0:T(8,128)(2,1)} %bitcast.7, ...), custom_call_target="tpu_custom_call" | custom-call | tf_op jit(solution)/shard_map/pallas_call | solution.py:513
  58.3 0.7 %copy.21 = bf16[384,256]{1,0:T(8,128)(2,1)} copy(bf16[384,256]{1,0:T(8,128)(2,1)S(1)} %shard_map.181) | data formatting | bytes 393216

commit v4 on v3

--- a/solution.py
+++ b/solution.py
@@ -45,9 +45,9 @@
     out_ref,
     feats, normed,
     wq, wrkv, wql, wkvl, wqc, wqrt, wku, wvu, wgw, wgl, trig,
-    colw, coll, kbuf, rvbuf, qbuf, ext, qwin, gatew, gatel,
+    colw, coll, kbuf, vbuf, rbuf, qbuf, ext, qwin, gatew, gatel,
     m_s, l_s, acc, o_send, st_send, o_recv, st_recv, wout, lat,
-    w_sem, fs_sem, fr_sem, ks_sem, kr_sem, vs_sem, vr_sem, qs_sem, qr_sem, ts_sem, tr_sem,
+    w_sem, fs_sem, fr_sem, ks_sem, kr_sem, vs_sem, vr_sem, rs_sem, rr_sem, hs_sem, hr_sem, qs_sem, qr_sem, ts_sem, tr_sem,
     bs_sem, br_sem, os_sem, or_sem, ss_sem, sr_sem, ws_sem, wr_sem, ls_sem, lr_sem,
 ):
     sp = lax.axis_index("sp")
@@ -147,26 +147,70 @@
             cp[name].wait_recv()
             cp[hand].start()
 
-    f_cp = spread(feats, fs_sem, fr_sem)
-    spread_first(f_cp)
-    spread_second(f_cp)
+    def direct(buf, ssem, rsem, lo=0, count=ROWS, first=0):
+        rows = pl.ds(lo, count)
+
+        def part(i, src, dst, dev):
+            return remote(buf.at[src, rows], buf.at[dst, rows], ssem.at[first + i], rsem.at[first + i], dev)
+
+        far, right, left = part(0, 0, 4, y_peer(2)), part(1, 0, 2, y_peer(1)), part(2, 0, 6, y_peer(-1))
+        own = part(3, 0, 1, sibling)
+        hands = [part(4, 2, 3, sibling), part(5, 6, 7, sibling), part(6, 4, 5, sibling)]
+        return [far, right, left, own], hands
+
+    def direct_first(cps):
+        for cp in cps[0]:
+            cp.start()
+
+    def direct_second(cps):
+        (far, right, left, own), hands = cps
+        for cp, hand in zip((right, left, far), hands):
+            cp.wait_recv()
+            hand.start()
+
+    f_cp = [spread(feats, fs_sem, fr_sem, p * 192, 192, p * 13) for p in range(2)]
+    for cp in f_cp:
+        spread_first(cp)
+    for cp in f_cp:
+        spread_second(cp)
 
     def squares(i):
         v = feats[i].astype(F32)
         v = v * v
         return v[:, :128] + v[:, 128:]
 
-    f_cp["sib"].wait_recv()
+    for cp in f_cp:
+        cp["sib"].wait_recv()
     total = squares(0) + squares(1) + squares(2) + squares(6)
-    for name in ("hlt", "hlb", "hrb", "hrt"):
-        f_cp[name].wait_recv()
-    total = total + squares(3) + squares(7)
-    spread_third(f_cp)
-    total = total + squares(4)
-    for name in ("hft", "hfb"):
-        f_cp[name].wait_recv()
+    for cp in f_cp:
+        spread_third(cp)
+    for cp in f_cp:
+        for name in ("hlt", "hlb", "hrb", "hrt"):
+            cp[name].wait_recv()
+    total = total + squares(3) + squares(7) + squares(4)
+    for cp in f_cp:
+        for name in ("hft", "hfb"):
+            cp[name].wait_recv()
     total = total + squares(5)
     inv = lax.rsqrt(jnp.sum(total, axis=-1, keepdims=True) * (1.0 / D) + EPS)
+
+    branch = {}
+    for slot in range(1, NTP):
+        dy, dc = slot // 2, slot % 2
+        peer = ((y + dy) % NY) * 2 + (c if dc == 0 else 1 - c)
+        cols = pl.ds(pl.multiple_of(peer * COLS, COLS), COLS)
+        i, j = slot - 1, slot + 6
+        branch[slot] = [
+            remote(wbw_h.at[:, cols], colw.at[slot], bs_sem.at[i], br_sem.at[i], (sp, peer)),
+            remote(wbl_h.at[:, cols], coll.at[slot], bs_sem.at[j], br_sem.at[j], (sp, peer)),
+        ]
+
+    def branch_start(*chosen):
+        for slot in chosen:
+            for cp in branch[slot]:
+                cp.start()
+
+    branch_start(1, 2, 6)
 
     for i in range(8):
         dy, dc = i // 2, i % 2
@@ -192,16 +236,35 @@
     loads[L_V].wait()
     lkv = rms(dot(normed[...], wkvl[...]), kvgain_ref)
     kbuf[0] = dot(lkv, wku[...]).astype(BF16)
-    rvbuf[0, 64:192] = jnp.transpose(dot(lkv, wvu[...])).astype(BF16)
+    vbuf[0] = jnp.transpose(dot(lkv, wvu[...])).astype(BF16)
     rkv = contract(normed[...], wrkv[...], 1, 1)
-    rvbuf[0, 0:64] = rotate_t(jnp.transpose(rkv[:, 0:64])).astype(BF16)
+    rbuf[0] = rotate_t(jnp.transpose(rkv[:, 0:64])).astype(BF16)
     ext[WINDOW:, :] = rkv[:, 64:192].astype(BF16)
 
     def k_copy(i, src, dst, dev):
-        return remote(kbuf.at[src], kbuf.at[dst], ks_sem.at[i], kr_sem.at[i], dev)
+        cuts = [pl.ds(h * (ROWS // 2), ROWS // 2) for h in range(2)]
+        return [
+            remote(kbuf.at[src, rows], kbuf.at[dst, rows], ks_sem.at[i * 2 + h], kr_sem.at[i * 2 + h], dev)
+            for h, rows in enumerate(cuts)
+        ]
 
     def v_copy(i, src, dst, dev):
-        return remote(rvbuf.at[src], rvbuf.at[dst], vs_sem.at[i], vr_sem.at[i], dev)
+        cuts = [pl.ds(h * (VDIM // 2), VDIM // 2) for h in range(2)]
+        return [
+            remote(vbuf.at[src, rows], vbuf.at[dst, rows], vs_sem.at[i * 2 + h], vr_sem.at[i * 2 + h], dev)
+            for h, rows in enumerate(cuts)
+        ]
+
+    mine = pl.ds(pl.multiple_of(c * (ROPE // 2), ROPE // 2), ROPE // 2)
+
+    def r_copy(i, src, dst, dev):
+        return [remote(rbuf.at[src, mine], rbuf.at[dst, mine], rs_sem.at[i], rr_sem.at[i], dev)]
+
+    r_hand = [
+        [remote(rbuf.at[slot, mine], rbuf.at[slot, mine], hs_sem.at[slot - 1], hr_sem.at[slot - 1], sibling)]
+        for slot in range(1, 8)
+    ]
+    useful = [None] + [z >= k for k in range(1, 4)] + [z + k >= NZ for k in range(1, 4)] + [z >= 4]
 
     up, down = z_peer(1), z_peer(-1)
     ups = [(0, 0, 1), (1, 1, 2), (2, 2, 3)]
@@ -211,6 +274,9 @@
     k_dn = [k_copy(*t, down) for t in downs]
     v_dn = [v_copy(*t, down) for t in downs]
     k_far = k_copy(6, 6, 7, down)
+    r_up = [r_copy(*t, up) for t in ups]
+    r_dn = [r_copy(*t, down) for t in downs]
+    r_far = r_copy(6, 6, 7, down)
     v_far = v_copy(6, 3, 7, up)
 
     def up_got(k):
@@ -225,28 +291,35 @@
     def v_down(k):
         return (z + k) % NZ <= 2
 
-    def when_start(cond, cp):
+    def when_start(cond, cps):
         @pl.when(cond)
         def _():
-            cp.start()
-
-    def when_recv(cond, cp):
+            for cp in cps:
+                cp.start()
+
+    def when_recv(cond, cps):
         @pl.when(cond)
         def _():
-            cp.wait_recv()
-
-    def when_sent(cond, cp):
+            for cp in cps:
+                cp.wait_recv()
+
+    def when_sent(cond, cps):
         @pl.when(cond)
         def _():
-            cp.wait_send()
+            for cp in cps:
+                cp.wait_send()
 
     when_start(up_go(0), k_up[0])
     when_start(k_down(0), k_dn[0])
+    when_start(up_go(0), r_up[0])
+    when_start(k_down(0), r_dn[0])
     when_start(up_go(0), v_up[0])
     when_start(v_down(0), v_dn[0])
 
     tail = remote(ext.at[pl.ds(ROWS, WINDOW)], ext.at[pl.ds(0, WINDOW)], ts_sem, tr_sem, sp_peer(1))
     tail.start()
+
+    branch_start(3, 7)
 
     loads[L_QL].wait()
     loads[L_QC].wait()
@@ -255,29 +328,14 @@
     qbuf[0:128, 0:ROWS] = jnp.transpose(dot(lq, wqc[...])).astype(BF16)
     qbuf[128:192, 0:ROWS] = rotate_t(contract(wqrt[...], lq, 1, 1)).astype(BF16)
     slots = [pl.ds(d * ROWS, ROWS) for d in range(NX)]
-    q_half = (pl.ds(0, 96), pl.ds(96, 96))
-
-    def q_copy(i, rows, src, dst, by):
-        return remote(
-            qbuf.at[rows, slots[src]], qbuf.at[rows, slots[dst]], qs_sem.at[i], qr_sem.at[i], x_peer(by)
-        )
-
-    q_all = pl.ds(0, NOPE + ROPE)
-    q_cp = [q_copy(0, q_all, 0, 1, 1), q_copy(1, q_all, 0, 3, -1)]
-    q_fwd = [q_copy(2, q_half[0], 1, 2, 1), q_copy(3, q_half[1], 3, 2, -1)]
+    q_cp = [
+        remote(qbuf.at[:, slots[0]], qbuf.at[:, slots[d]], qs_sem.at[d - 1], qr_sem.at[d - 1], x_peer(d))
+        for d in (2, 1, 3)
+    ]
     for cp in q_cp:
         cp.start()
 
-    branch = []
-    for slot in range(1, NTP):
-        dy, dc = slot // 2, slot % 2
-        peer = ((y + dy) % NY) * 2 + (c if dc == 0 else 1 - c)
-        cols = pl.ds(pl.multiple_of(peer * COLS, COLS), COLS)
-        i, j = slot - 1, slot + 6
-        branch.append(remote(wbw_h.at[:, cols], colw.at[slot], bs_sem.at[i], br_sem.at[i], (sp, peer)))
-        branch.append(remote(wbl_h.at[:, cols], coll.at[slot], bs_sem.at[j], br_sem.at[j], (sp, peer)))
-    for cp in branch:
-        cp.start()
+    branch_start(4)
 
     loads[L_Q].wait()
     qwin[...] = dot(normed[...], wq[...]).astype(BF16)
@@ -307,9 +365,9 @@
             p = (w / den).astype(BF16)
             o = contract(p, kv[:, 64:128], 0, 0).astype(BF16)
             wout[0, lo : lo + 128, :] = jnp.concatenate([o[:128], o[128:]], axis=1)
-        spread_first(w_cp)
-
-    w_cp = spread(wout, ws_sem, wr_sem)
+        direct_first(w_cp)
+
+    w_cp = direct(wout, ws_sem, wr_sem)
 
     m_s[...] = jnp.full((1, NX * ROWS), NEGATIVE, F32)
     l_s[...] = jnp.zeros((1, NX * ROWS), F32)
@@ -330,62 +388,76 @@
         acc[:, cols] = acc[:, cols] * alpha + dot(vals, p.astype(BF16))
 
     def block(slot):
-        keys = jnp.concatenate([kbuf[slot], jnp.transpose(rvbuf[slot, 0:64])], axis=1)
-        return keys, rvbuf[slot, 64:192]
-
-    def whole(slot, useful):
-        @pl.when(useful)
+        keys = jnp.concatenate([kbuf[slot], jnp.transpose(rbuf[slot])], axis=1)
+        return keys, vbuf[slot]
+
+    def whole(slot):
+        @pl.when(useful[slot])
         def _():
+            r_hand[slot - 1][0].wait_recv()
             keys, vals = block(slot)
             tile(keys, vals, pl.ds(0, NX * ROWS), False)
 
-    def own():
+    def own_square():
         keys, vals = block(0)
         tile(keys, vals, slots[0], True)
+
+    def own_rest():
+        keys, vals = block(0)
         for d in range(1, NX):
 
             @pl.when(d > x)
             def _():
                 tile(keys, vals, slots[d], False)
 
+    def relay(got, arrived, go, onward):
+        for i, cp in enumerate(arrived):
+            when_recv(got, [cp])
+            if onward is not None:
+                when_start(go, [onward[i]])
+
     def relay_k(k):
-        when_recv(up_got(k), k_up[k - 1])
-        if k < 3:
-            when_start(up_go(k), k_up[k])
-        when_recv(k_down(k), k_dn[k - 1])
-        when_start(k_down(k), k_dn[k] if k < 3 else k_far)
+        more = k < 3
+        for h in range(2):
+            relay(up_got(k), k_up[k - 1][h : h + 1], up_go(k), k_up[k][h : h + 1] if more else None)
+            relay(k_down(k), k_dn[k - 1][h : h + 1], k_down(k), (k_dn[k] if more else k_far)[h : h + 1])
+        relay(up_got(k), r_up[k - 1], up_go(k), r_up[k] if more else None)
+        when_start(useful[k], r_hand[k - 1])
+        relay(k_down(k), r_dn[k - 1], k_down(k), r_dn[k] if more else r_far)
+        when_start(useful[k + 3], r_hand[k + 2])
 
     def relay_v(k):
-        when_recv(up_got(k), v_up[k - 1])
-        when_start(up_go(k), v_up[k] if k < 3 else v_far)
-        when_recv(v_down(k), v_dn[k - 1])
-        if k < 3:
-            when_start(v_down(k), v_dn[k])
+        for h in range(2):
+            relay(up_got(k), v_up[k - 1][h : h + 1], up_go(k), v_up[k][h : h + 1])
+            relay(v_down(k), v_dn[k - 1][h : h + 1], v_down(k), v_dn[k][h : h + 1])
 
     relay_k(1)
+    own_square()
     relay_v(1)
-    for cp, nxt in zip(q_cp, q_fwd):
+    branch_start(5)
+    relay_k(2)
+    windowed()
+    relay_v(2)
+    for cp in q_cp:
         cp.wait_recv()
-        nxt.start()
-    windowed()
-    relay_k(2)
-    for cp in q_fwd:
-        cp.wait_recv()
-    own()
-    relay_v(2)
-    whole(1, z >= 1)
+    own_rest()
+    whole(1)
     relay_k(3)
-    whole(4, z >= 7)
-    spread_second(w_cp)
-    relay_v(3)
-    whole(2, z >= 2)
-    whole(5, z >= 6)
-    spread_third(w_cp)
-    whole(3, z >= 3)
-    whole(6, z >= 5)
+    for h in range(2):
+        relay((z >= 3) & (z < NZ - 1), v_up[2][h : h + 1], up_go(3), v_far[h : h + 1])
+    whole(4)
+    whole(2)
+    when_recv(z == NZ - 1, v_up[2])
+    when_recv(v_down(3), v_dn[2])
+    direct_second(w_cp)
+    whole(5)
+    whole(3)
+    whole(6)
     when_recv(z >= 4, k_far)
+    when_recv(z >= 4, r_far)
+    when_start(z >= 4, r_hand[6])
     when_recv(z >= 4, v_far)
-    whole(7, z >= 4)
+    whole(7)
 
     pieces = [pl.ds(p * 128, 128) for p in range(3)]
     st_cp, o_cp = [], [[], [], []]
@@ -402,16 +474,17 @@
             o_cp[p].append(remote(o_send.at[i], o_recv.at[i], os_sem.at[i], or_sem.at[i], x_peer(-d)))
             o_cp[p][-1].start()
 
-    for cp in branch:
+    blocks = [cp for slot in range(1, NTP) for cp in branch[slot]]
+    for cp in blocks:
         cp.wait_recv()
     loads[L_BW].wait()
     loads[L_BL].wait()
-    for name in ("sib", "hlt", "hlb", "hrb", "hrt", "hft", "hfb"):
-        w_cp[name].wait_recv()
+    for cp in [w_cp[0][3]] + w_cp[1]:
+        cp.wait_recv()
     allw = jnp.concatenate([wout[d] for d in range(NTP)], axis=1)
     gatew[...] = gatew[...] * dot(allw, colw[...].reshape(NTP * 128, COLS))
 
-    l_cp = [spread(lat, ls_sem, lr_sem, p * 128, 128, p * 13) for p in range(3)]
+    l_cp = [direct(lat, ls_sem, lr_sem, p * 128, 128, p * 7) for p in range(3)]
     for cp in st_cp:
         cp.wait_recv()
     for p, cols in enumerate(pieces):
@@ -426,11 +499,11 @@
         for d in range(3):
             o = o + o_recv[d * 3 + p].astype(F32) * ws[d + 1]
         lat[0, cols] = jnp.transpose(o / den).astype(BF16)
-        spread_first(l_cp[p])
+        direct_first(l_cp[p])
     for cp in l_cp:
-        spread_second(cp)
+        direct_second(cp)
     for cp in l_cp:
-        cp["sib"].wait_recv()
+        cp[0][3].wait_recv()
 
     def branch_part(first, count):
         rows = jnp.concatenate([lat[i] for i in range(first, first + count)], axis=1)
@@ -438,26 +511,28 @@
 
     mixed = branch_part(0, 2)
     for cp in l_cp:
-        spread_third(cp)
-    for cp in l_cp:
-        for name in ("hlt", "hlb", "hrb", "hrt"):
-            cp[name].wait_recv()
+        cp[1][0].wait_recv()
+        cp[1][1].wait_recv()
     mixed = mixed + branch_part(2, 2) + branch_part(6, 2)
     for cp in l_cp:
-        for name in ("hft", "hfb"):
-            cp[name].wait_recv()
+        cp[1][2].wait_recv()
     mixed = mixed + branch_part(4, 2)
     out_ref[...] = (gatew[...] + gatel[...] * mixed).astype(BF16)
 
-    sent = list(f_cp.values()) + list(w_cp.values()) + branch + q_cp + q_fwd + [tail] + st_cp
+    sent = list(f_cp[0].values()) + list(f_cp[1].values()) + w_cp[0] + w_cp[1] + blocks + q_cp + [tail] + st_cp
     for p in range(3):
-        sent += list(l_cp[p].values()) + o_cp[p]
+        sent += l_cp[p][0] + l_cp[p][1] + o_cp[p]
     for k in range(3):
         when_sent(up_go(k), k_up[k])
         when_sent(up_go(k), v_up[k])
         when_sent(k_down(k), k_dn[k])
         when_sent(v_down(k), v_dn[k])
+        when_sent(up_go(k), r_up[k])
+        when_sent(k_down(k), r_dn[k])
+    for slot in range(1, 8):
+        when_sent(useful[slot], r_hand[slot - 1])
     when_sent(k_down(3), k_far)
+    when_sent(k_down(3), r_far)
     when_sent(up_go(3), v_far)
     for cp in sent:
         cp.wait_send()
@@ -489,7 +564,8 @@
         pltpu.VMEM((NTP, 128, COLS), BF16),
         pltpu.VMEM((NTP, 128, COLS), BF16),
         pltpu.VMEM((8, ROWS, NOPE), BF16),
-        pltpu.VMEM((8, ROPE + VDIM, ROWS), BF16),
+        pltpu.VMEM((8, VDIM, ROWS), BF16),
+        pltpu.VMEM((8, ROPE, ROWS), BF16),
         pltpu.VMEM((NOPE + ROPE, NX * ROWS), BF16),
         pltpu.VMEM((ROWS + WINDOW, 128), BF16),
         pltpu.VMEM((ROWS, 128), BF16),
@@ -506,9 +582,9 @@
         pltpu.VMEM((NTP, ROWS, 128), BF16),
     ]
     scratch += [
-        dma((15,)), dma((13,)), dma((13,)), dma((7,)), dma((7,)), dma((7,)), dma((7,)),
+        dma((15,)), dma((26,)), dma((26,))] + [dma((14,))] * 4 + [dma((7,))] * 4 + [
         dma((4,)), dma((4,)), dma(()), dma(()), dma((14,)), dma((14,)),
-        dma((9,)), dma((9,)), dma((3,)), dma((3,)), dma((13,)), dma((13,)), dma((39,)), dma((39,)),
+        dma((9,)), dma((9,)), dma((3,)), dma((3,)), dma((7,)), dma((7,)), dma((21,)), dma((21,)),
     ]
     return pl.pallas_call(
         layer,

time: 60.1 us -> 58.4 us (0.972)
  the two profiles are of different devices: /device:TPU:3 before, /device:TPU:193 now
where the time goes in v4:
time: 58.4 us; the launch traced here: 58.3 us
  Pallas kernels  57.6 us (99%)
  local copies, waits for them, and re-layouts  0.68 us (1%)
    pallas_call x1, Pallas kernels, on_device(): pl.pallas_call(layer, out_shape=pltpu.VMEM((ROWS, COLS), BF16), in_specs=...  57.6 us

profile of v4, /device:TPU:193, one launch (start us, length us, event | category | flops | bytes accessed | tf_op | source)
XLA Modules:
  0.0 58.3 jit_solution(8572212419701376550)
XLA Ops:
  0.0 57.6 %shard_map.181 = bf16[384,256]{1,0:T(8,128)(2,1)S(1)} custom-call(bf16[384,256]{1,0:T(8,128)(2,1)} %x_ref.1, f32[1,2048]{1,0:T(1,128)} %bitcast.11, f32[1,512]{1,0:T(1,128)} %bitcast.12, f32[1,512]{1,0:T(1,128)} %bitcast.13, f32[2]{0:T(128)} %sink_ref.1, bf16[2048,128]{1,0:T(8,128)(2,1)} %wq_h.1, bf16[64,2048]{1,0:T(8,128)(2,1)} %bitcast.7, ...), custom_call_target="tpu_custom_call" | custom-call | tf_op jit(solution)/shard_map/pallas_call | solution.py:589
  57.7 0.7 %copy.21 = bf16[384,256]{1,0:T(8,128)(2,1)} copy(bf16[384,256]{1,0:T(8,128)(2,1)S(1)} %shard_map.181) | data formatting | bytes 393216
